TPU v7x, 32 devices: a whole 2x2x4 slice. The times are simulated.
32 devices in a mesh: sp: 8 (over z, x), tp: 4 (over y, core).
Axes of the slice: x: 2, y: 2, z: 4, core: 2. Of those that a mesh axis runs over, the one named last changes fastest.
Arguments:
- tokens: bfloat16 [8192, 2048], P('sp', 'tp'), may hold values from -16 to 16
- norm_gain: float32 [2048], replicated, may hold values from 0.1 to 1.9
- signal_proj: bfloat16 [2048, 1024], P(None, 'tp'), may hold values from -0.125 to 0.125
- postgate_proj: bfloat16 [2048, 1024], P(None, 'tp'), may hold values from -0.125 to 0.125
- pregate_proj: bfloat16 [2048, 1024], P(None, 'tp'), may hold values from -0.125 to 0.125
- query_proj: bfloat16 [2048, 1024], P(None, 'tp'), may hold values from -0.21875 to 0.21875
- key_proj: bfloat16 [2048, 1024], P(None, 'tp'), may hold values from -0.21875 to 0.21875
- value_proj: bfloat16 [2048, 1024], P(None, 'tp'), may hold values from -0.125 to 0.125
- filter_taps: bfloat16 [3, 1024], P(None, 'tp'), may hold values from -3.5 to 3.5
- break_bias: bfloat16 [8192, 16], P('sp', 'tp'), may hold values from -18 to 0
- filter_readout: bfloat16 [1024, 2048], replicated, may hold values from -0.125 to 0.125
- attention_readout: bfloat16 [1024, 2048], replicated, may hold values from -0.125 to 0.125
Outputs:
- mixed: bfloat16 [8192, 2048], P(('sp', 'tp'))
- mass_logarithm: float32 [16, 8192], P('tp', 'sp')
All inputs are finite; a program needn't handle non-finite values.
Results may differ from a plain program's by a relative error of at most 0.013.
Values may be sent and summed in bfloat16 or wider, within the bound.
A program may use at most 128 MiB of HBM per device.

v0:
```python
import functools

import jax
import jax.numpy as jnp
from jax import lax
from jax.experimental import pallas as pl
from jax.experimental.pallas import tpu as pltpu
from jax.sharding import PartitionSpec as P

HEAD_DIM = 64
CONV_W = 3
KEY_CHUNK = 256


epsilon = 1e-06
mass_floor = 0.1
score_cap = 88.0


def passed_along(block, axis, distance):
    devices = range(lax.axis_size(axis))
    route = [(i - distance, i) for i in devices if i - distance in devices]
    return lax.ppermute(block, axis, route)


def attention_kernel(tok_dev, share, rows, chain, part_ref, recv_ref, bias_ref, out_ref, acc, carry):
    chunk = KEY_CHUNK
    tile = pl.program_id(0)
    tiles_block = share // rows
    block = tile // tiles_block
    inner = (tile % tiles_block) * rows
    row_start = block * tok_dev + part_ref[0] * share + inner
    chunks_block = tok_dev // chunk
    acc[...] = jnp.zeros_like(acc)
    carry[...] = jnp.zeros_like(carry)
    later = lax.broadcasted_iota(jnp.int32, (chunk, chunk), 0)
    earlier = lax.broadcasted_iota(jnp.int32, (chunk, chunk), 1)
    after = jnp.where(later > earlier, 1.0, 0.0).astype(jnp.bfloat16)

    def step(masked, index):
        offset = pl.multiple_of((index % chunks_block) * chunk, chunk)
        key_value = recv_ref[index // chunks_block, pl.ds(offset, chunk), :]
        bias = bias_ref[index]
        for link in range(rows // chain):
            place = pl.ds(link * chain, chain)
            query_place = pl.multiple_of(tok_dev + inner + link * chain, chain)
            query = recv_ref[block, pl.ds(query_place, chain), :]
            scores = lax.dot_general(
                query, key_value, (((1,), (1,)), ((), ())), preferred_element_type=jnp.float32
            )
            scores = jnp.minimum(scores + bias, score_cap)
            lost = jnp.log(1.0 + jnp.exp(scores))
            own = scores - lost
            if masked:
                row_ids = lax.broadcasted_iota(jnp.int32, scores.shape, 0) + (row_start + link * chain)
                col_ids = lax.broadcasted_iota(jnp.int32, scores.shape, 1) + index * chunk
                allowed = col_ids < row_ids
                lost = jnp.where(allowed, lost, 0.0)
            behind = jnp.dot(lost.astype(jnp.bfloat16), after, preferred_element_type=jnp.float32)
            before = carry[place, :]
            weights = jnp.exp(own - (behind + before))
            if masked:
                weights = jnp.where(allowed, weights, 0.0)
            acc[place, :] += jnp.dot(
                weights.astype(jnp.bfloat16), key_value, preferred_element_type=jnp.float32
            )
            carry[place, :] = before + (behind[:, :1] + lost[:, :1])

    full = row_start // chunk
    top = (row_start + rows + chunk - 1) // chunk

    @pl.loop(0, top - full)
    def _(i):
        step(True, top - 1 - i)

    @pl.loop(0, full)
    def _(i):
        step(False, full - 1 - i)

    remain = jnp.broadcast_to(-carry[...], acc.shape)
    high = remain.astype(jnp.bfloat16)
    rest = remain - high.astype(jnp.float32)
    middle = rest.astype(jnp.bfloat16)
    low = (rest - middle.astype(jnp.float32)).astype(jnp.bfloat16)
    lane = lax.broadcasted_iota(jnp.int32, acc.shape, 1)
    packed = jnp.where(lane == 0, high.astype(jnp.float32), 0.0)
    packed = jnp.where(lane == 1, middle.astype(jnp.float32), packed)
    packed = jnp.where(lane == 2, low.astype(jnp.float32), packed)
    out_ref[0] = jnp.where(lane >= HEAD_DIM, acc[...], packed).astype(jnp.bfloat16)


def attend(received, bias_row, part, tok_dev):
    n_sp, _, lanes = received.shape
    share = received.shape[1] - tok_dev
    rows = min(512, share)
    chain = min(256, rows)
    tiles_block = share // rows
    bias3 = bias_row.reshape(n_sp * tok_dev // KEY_CHUNK, 1, KEY_CHUNK)
    pairs = n_sp * share * n_sp * tok_dev // 2
    return pl.pallas_call(
        functools.partial(attention_kernel, tok_dev, share, rows, chain),
        out_shape=jax.ShapeDtypeStruct((n_sp, share, lanes), jnp.bfloat16),
        grid_spec=pltpu.PrefetchScalarGridSpec(
            num_scalar_prefetch=1,
            grid=(n_sp * tiles_block,),
            in_specs=[
                pl.BlockSpec(received.shape, lambda i, part: (0, 0, 0)),
                pl.BlockSpec(bias3.shape, lambda i, part: (0, 0, 0)),
            ],
            out_specs=pl.BlockSpec((1, rows, lanes), lambda i, part: (i // tiles_block, i % tiles_block, 0)),
            scratch_shapes=[
                pltpu.VMEM((rows, lanes), jnp.float32),
                pltpu.VMEM((rows, 1), jnp.float32),
            ],
        ),
        compiler_params=pltpu.CompilerParams(
            dimension_semantics=("arbitrary",), vmem_limit_bytes=32 * 1024 * 1024
        ),
        cost_estimate=pl.CostEstimate(
            flops=pairs * (4 * lanes + 2 * KEY_CHUNK), bytes_accessed=received.size * 2, transcendentals=3 * pairs
        ),
    )(part, received, bias3)


def per_device(
    tokens,
    norm_gain,
    signal_proj,
    postgate_proj,
    pregate_proj,
    query_proj,
    key_proj,
    value_proj,
    filter_taps,
    break_bias,
    filter_readout,
    attention_readout,
):
    tok_dev = tokens.shape[0]
    heads_dev = break_bias.shape[1]
    n_sp = lax.axis_size("sp")
    parts = n_sp // heads_dev
    share = tok_dev // parts
    position = lax.axis_index("sp")
    all_bias = lax.all_gather(break_bias.T, "sp", axis=1, tiled=True)
    all_bias, tokens = lax.optimization_barrier((all_bias, tokens))
    bias_row = lax.dynamic_slice_in_dim(all_bias, position // parts, 1, 0).astype(jnp.float32)
    model = key_proj.shape[0]
    key_value_proj = jnp.concatenate(
        [
            key_proj.reshape(model, heads_dev, HEAD_DIM),
            value_proj.reshape(model, heads_dev, HEAD_DIM),
        ],
        axis=2,
    ).reshape(model, 2 * heads_dev * HEAD_DIM)
    whole_rows = lax.all_gather(tokens, "tp", axis=1, tiled=True)
    widened = whole_rows.astype(jnp.float32)
    inverse = lax.rsqrt(jnp.mean(widened * widened, axis=1) + epsilon)
    scaled = (widened * norm_gain[None, :]).astype(jnp.bfloat16)

    def project(weight, factor=1.0):
        product = jnp.dot(scaled, weight, preferred_element_type=jnp.float32)
        return (product * inverse[:, None]).astype(jnp.bfloat16) * jnp.bfloat16(factor)

    key_values = project(key_value_proj).reshape(tok_dev, heads_dev, 2 * HEAD_DIM)
    queries = project(query_proj, HEAD_DIM ** (-0.5)).reshape(tok_dev, heads_dev, HEAD_DIM)
    queries = jnp.pad(queries, ((0, 0), (0, 0), (0, HEAD_DIM)))
    key_values = key_values.transpose(1, 0, 2)
    queries = queries.transpose(1, 0, 2)
    outgoing = jnp.stack(
        [
            jnp.concatenate([key_values, queries[:, part * share : (part + 1) * share]], axis=1)
            for part in range(parts)
        ],
        axis=1,
    ).reshape(n_sp, tok_dev + share, 2 * HEAD_DIM)
    received = lax.all_to_all(outgoing, "sp", split_axis=0, concat_axis=0, tiled=True)
    signal, post_gate, pre_gate = (project(w) for w in (signal_proj, postgate_proj, pregate_proj))
    rim_width = CONV_W - 1
    rim_signal, rim_pre = passed_along(
        (signal[tok_dev - rim_width :], pre_gate[tok_dev - rim_width :]), "sp", 1
    )
    extended = jnp.concatenate(
        [
            rim_pre.astype(jnp.float32) * rim_signal.astype(jnp.float32),
            pre_gate.astype(jnp.float32) * signal.astype(jnp.float32),
        ],
        axis=0,
    )
    tap_values = filter_taps.astype(jnp.float32)
    running = jnp.zeros((tok_dev, extended.shape[1]), jnp.float32)
    for offset in range(CONV_W):
        running = running + tap_values[offset][None, :] * extended[offset : offset + tok_dev]
    filtered = (post_gate.astype(jnp.float32) * running).astype(jnp.bfloat16)
    filter_rows = lax.all_to_all(filtered, "tp", split_axis=0, concat_axis=1, tiled=True)

    part = (position % parts).astype(jnp.int32).reshape(1)
    computed = attend(received, bias_row, part, tok_dev)
    returned = lax.all_to_all(computed, "sp", split_axis=0, concat_axis=0, tiled=True)
    returned = returned.reshape(heads_dev, tok_dev, 2 * HEAD_DIM)
    attended = returned[:, :, HEAD_DIM:].transpose(1, 0, 2).reshape(tok_dev, heads_dev * HEAD_DIM)
    remain = jnp.sum(returned[:, :, :3].astype(jnp.float32), axis=2)
    mass_logarithm = jnp.log(jnp.maximum(-jnp.expm1(remain), mass_floor))
    attended_rows = lax.all_to_all(attended, "tp", split_axis=0, concat_axis=1, tiled=True)
    mixed = (
        jnp.dot(filter_rows, filter_readout, preferred_element_type=jnp.float32)
        + jnp.dot(attended_rows, attention_readout, preferred_element_type=jnp.float32)
    ).astype(jnp.bfloat16)
    return (mixed, mass_logarithm)


def solution(mesh):
    placed = (
        P("sp", "tp"),
        P(),
        P(None, "tp"),
        P(None, "tp"),
        P(None, "tp"),
        P(None, "tp"),
        P(None, "tp"),
        P(None, "tp"),
        P(None, "tp"),
        P("sp", "tp"),
        P(),
        P(),
    )
    return jax.shard_map(
        per_device,
        mesh=mesh,
        in_specs=placed,
        out_specs=(P(("sp", "tp"), None), P("tp", "sp")),
        check_vma=False,
    )
```

profile of v0, /device:TPU:15, one launch (start us, length us, event | category | flops | bytes accessed | tf_op | source)
XLA Modules:
  0.0 335.8 jit_solution(6553158198936285968)
XLA Ops:
  7.2 22.2 %all_gather.6 = bf16[4,8192]{1,0:T(4,128)(2,1)S(1)} all-gather(bf16[4,1024]{1,0:T(4,128)(2,1)} %bitcast.56), channel_id=1, replica_groups=mesh['sp'=8,'tp'=4] {'sp'}, dimensions={1}, use_global_device_ids=true | all-gather | bytes 73728 | tf_op jit(solution)/shard_map/all_gather | solution.py:145
  29.4 1.5 copy.30
  32.4 1.5 pad_maximum_fusion.1
  33.9 39.4 %all-gather.2.cloned.1.call-done = bf16[1024,2048]{1,0:T(8,128)(2,1)} async-done(((bf16[1024,512]{1,0:T(8,128)(2,1)}), bf16[1024,2048]{1,0:T(8,128)(2,1)}) %all-gather.2.cloned.1.call-update) | async-done | bytes 4194320 | tf_op jit(solution)/shard_map/all_gather | solution.py:156
  73.3 3.2 fusion.1
  76.8 2.5 fusion.50
  80.2 6.2 %multiply_convert_fusion = bf16[1024,512]{0,1:T(8,128)(2,1)} fusion(bf16[2048,512]{0,1:T(8,128)(2,1)} %bitcast.50, bf16[1024,2048]{1,0:T(8,128)(2,1)} %all-gather.2.cloned.1.call-done, f32[2048]{0:T(1024)S(1)} %copy-done.5, f32[1024]{0:T(1024)S(1)} %add_rsqrt_fusion), kind=kOutput, calls=%fused_computation.14 | convolution fusion | flops 2154823680 | bytes 7352320 | tf_op jit(solution)/shard_map/dot_general | solution.py:162
  86.5 1.6 copy.32
  88.4 2.0 pad_maximum_fusion
  90.5 5.6 %all-to-all-start.1 = ((bf16[8,1536,128]{2,1,0:T(8,128)(2,1)}), bf16[8,1536,128]{2,1,0:T(8,128)(2,1)}, u32[]{:S(2)}, u32[]{:S(2)}) async-start(bf16[8,1536,128]{2,1,0:T(8,128)(2,1)} %bitcast.42), calls=%async_computation.1 | async-start | bytes 6291456 | tf_op jit(solution)/shard_map/all_to_all | solution.py:177
  96.1 3.6 %fusion.35 = bf16[1024,256]{1,0:T(8,128)(2,1)S(1)} fusion(bf16[2048,256]{1,0:T(8,128)(2,1)S(1)} %copy-done.4, bf16[1024,2048]{1,0:T(8,128)(2,1)} %all-gather.2.cloned.1.call-done, f32[2048]{0:T(1024)S(1)} %copy-done.5, f32[1024]{0:T(1024)S(1)} %add_rsqrt_fusion), kind=kOutput, calls=%fused_computation.25 | convolution fusion | flops 1080557568 | bytes 5779456 | tf_op jit(solution)/shard_map/dot_general | solution.py:162
  99.8 2.3 convert_multiply_fusion.2
  102.1 3.1 collective-permute-start.1
  105.2 3.1 collective-permute-start
  108.3 55.9 %collective-permute-done.1 = bf16[2,256]{1,0:T(2,128)(2,1)S(1)} collective-permute-done((bf16[2,256]{1,0:T(2,128)(2,1)S(1)}, bf16[2,256]{1,0:T(2,128)(2,1)S(1)}, u32[]{:S(2)}, u32[]{:S(2)}) %collective-permute-start.1) | collective-permute-done | bytes 1056 | tf_op jit(solution)/shard_map/ppermute | solution.py:23
  164.3 5.0 %fusion.47 = bf16[1024,256]{1,0:T(8,128)(2,1)S(1)} fusion(bf16[2048,256]{1,0:T(8,128)(2,1)} %param.15, bf16[1024,2048]{1,0:T(8,128)(2,1)} %all-gather.2.cloned.1.call-done, f32[2048]{0:T(1024)S(1)} %copy-done.5, f32[2,256]{1,0:T(2,128)S(1)} %convert_multiply_fusion.3, f32[1024,256]{1,0:T(8,128)} %get-tuple-element.13, f32[256]{0:T(256)S(1)} %bitcast.59, ...), kind=kOutput, calls=%fused_computation.29 | convolution fusion | flops 1083179008 | bytes 6833152 | tf_op jit(solution)/shard_map/dot_general | solution.py:162
  170.2 5.0 %all-to-all-start = ((bf16[4,256,256]{1,2,0:T(8,128)(2,1)}), bf16[4,256,256]{1,2,0:T(8,128)(2,1)S(1)}, u32[]{:S(2)}, u32[]{:S(2)}) async-start(bf16[4,256,256]{1,2,0:T(8,128)(2,1)} %copy.29), calls=%async_computation | async-start | bytes 1048576 | tf_op jit(solution)/shard_map/all_to_all | solution.py:195
  175.3 107.0 %shard_map.131 = bf16[8,512,128]{2,1,0:T(8,128)(2,1)} custom-call(s32[1]{0:T(128)} %bitcast.7.part_ref, bf16[8,1536,128]{2,1,0:T(8,128)(2,1)} %all-to-all-done.1.recv_ref, f32[32,1,256]{2,1,0:T(1,128)S(1)} %convert.1.bias_ref), custom_call_target="tpu_custom_call" | custom-call | flops 17179869184 | bytes 3145728 | tf_op jit(solution)/shard_map/pallas_call | solution.py:100
  282.3 3.6 %all-to-all-start.2 = ((bf16[8,512,128]{2,1,0:T(8,128)(2,1)}), bf16[8,512,128]{2,1,0:T(8,128)(2,1)S(1)}, u32[]{:S(2)}, u32[]{:S(2)}) async-start(bf16[8,512,128]{2,1,0:T(8,128)(2,1)} %shard_map.131), calls=%async_computation.2 | async-start | bytes 2097152 | tf_op jit(solution)/shard_map/all_to_all | solution.py:199
  285.9 4.8 %fusion.60 = f32[256,2048]{1,0:T(8,128)} fusion(bf16[256,1024]{0,1:T(8,128)(2,1)S(1)} %bitcast.52, bf16[1024,2048]{1,0:T(8,128)(2,1)} %param.22), kind=kOutput, calls=%fused_computation.47 | convolution fusion | flops 1073741824 | bytes 6815744 | tf_op jit(solution)/shard_map/dot_general | solution.py:206
  290.7 18.4 %all-to-all-done.2 = bf16[8,512,128]{2,1,0:T(8,128)(2,1)S(1)} async-done(((bf16[8,512,128]{2,1,0:T(8,128)(2,1)}), bf16[8,512,128]{2,1,0:T(8,128)(2,1)S(1)}, u32[]{:S(2)}, u32[]{:S(2)}) %all-to-all-start.2) | async-done | bytes 1048608 | tf_op jit(solution)/shard_map/all_to_all | solution.py:199
  312.9 3.9 %all-to-all-start.3 = ((bf16[4,256,256]{1,2,0:T(8,128)(2,1)}), bf16[4,256,256]{1,2,0:T(8,128)(2,1)S(1)}, u32[]{:S(2)}, u32[]{:S(2)}) async-start(bf16[4,256,256]{1,2,0:T(8,128)(2,1)} %copy.39), calls=%async_computation.3 | async-start | bytes 1048576 | tf_op jit(solution)/shard_map/all_to_all | solution.py:204
  317.9 6.0 %all-to-all-done.3 = bf16[4,256,256]{1,2,0:T(8,128)(2,1)S(1)} async-done(((bf16[4,256,256]{1,2,0:T(8,128)(2,1)}), bf16[4,256,256]{1,2,0:T(8,128)(2,1)S(1)}, u32[]{:S(2)}, u32[]{:S(2)}) %all-to-all-start.3) | async-done | bytes 524320 | tf_op jit(solution)/shard_map/all_to_all | solution.py:204
  323.8 5.1 %fusion.2 = bf16[256,2048]{1,0:T(8,128)(2,1)} fusion(f32[256,2048]{1,0:T(8,128)} %fusion.60, bf16[256,1024]{0,1:T(8,128)(2,1)S(1)} %bitcast.53, bf16[1024,2048]{1,0:T(8,128)(2,1)} %param.23), kind=kOutput, calls=%fused_computation.6 | convolution fusion | flops 1074790400 | bytes 7864320 | tf_op jit(solution)/shard_map/dot_general | solution.py:207
  (38 shorter events, 9.0 us)
Async XLA Ops:
  7.2 92.6 %copy-start = (bf16[2048,256]{1,0:T(8,128)(2,1)S(1)}, bf16[2048,256]{1,0:T(8,128)(2,1)}, u32[]{:S(2)}) copy-start(bf16[2048,256]{1,0:T(8,128)(2,1)} %param.14) | copy-start | bytes 3145732
  7.2 66.1 %all-gather.2.cloned.1.call-start = ((), (), s32[]{:S(2)}) async-start(), calls=%async_computation.4 | async-start | bytes 5242880 | tf_op jit(solution)/shard_map/all_gather | solution.py:156
  32.4 44.2 %copy-start.5 = (f32[2048]{0:T(1024)S(1)}, f32[2048]{0:T(1024)}, u32[]{:S(2)}) copy-start(f32[2048]{0:T(1024)} %param.13) | copy-start | bytes 24580
  73.3 3.4 %copy-start.1 = (bf16[1024,2048]{1,0:T(8,128)(2,1)S(1)}, bf16[1024,2048]{1,0:T(8,128)(2,1)}, u32[]{:S(2)}) copy-start(bf16[1024,2048]{1,0:T(8,128)(2,1)} %all-gather.2.cloned.1.call-done) | copy-start | bytes 12582916
  90.4 5.7 %copy-start.4 = (bf16[2048,256]{1,0:T(8,128)(2,1)S(1)}, bf16[2048,256]{1,0:T(8,128)(2,1)}, u32[]{:S(2)}) copy-start(bf16[2048,256]{1,0:T(8,128)(2,1)} %param.16) | copy-start | bytes 3145732
  90.5 79.8 %all-to-all-start.1 = ((bf16[8,1536,128]{2,1,0:T(8,128)(2,1)}), bf16[8,1536,128]{2,1,0:T(8,128)(2,1)}, u32[]{:S(2)}, u32[]{:S(2)}) async-start(bf16[8,1536,128]{2,1,0:T(8,128)(2,1)} %bitcast.42), calls=%async_computation.1 | async-start | bytes 6291456 | tf_op jit(solution)/shard_map/all_to_all | solution.py:177
  96.1 3.7 %copy-start.2 = (bf16[1024,2048]{1,0:T(8,128)(2,1)S(1)}, bf16[1024,2048]{1,0:T(8,128)(2,1)}, u32[]{:S(2)}) copy-start(bf16[1024,2048]{1,0:T(8,128)(2,1)} %all-gather.2.cloned.1.call-done) | copy-start | bytes 12582916
  99.8 8.5 %copy-start.3 = (bf16[3,256]{1,0:T(4,128)(2,1)S(1)}, bf16[3,256]{1,0:T(4,128)(2,1)}, u32[]{:S(2)}) copy-start(bf16[3,256]{1,0:T(4,128)(2,1)} %param.20) | copy-start | bytes 4612
  102.1 62.2 %collective-permute-start.1 = (bf16[2,256]{1,0:T(2,128)(2,1)S(1)}, bf16[2,256]{1,0:T(2,128)(2,1)S(1)}, u32[]{:S(2)}, u32[]{:S(2)}) collective-permute-start(bf16[2,256]{1,0:T(2,128)(2,1)S(1)} %slice.46), channel_id=1, source_target_pairs={{0,4},{4,8},{8,12},{12,16},{16,20},{20,24},{24,28},{1,5},{5,9},{9,... | collective-permute-start | bytes 3080 | tf_op jit(solution)/shard_map/ppermute | solution.py:23
  105.2 59.1 %collective-permute-start = (bf16[2,256]{1,0:T(2,128)(2,1)S(1)}, bf16[2,256]{1,0:T(2,128)(2,1)S(1)}, u32[]{:S(2)}, u32[]{:S(2)}) collective-permute-start(bf16[2,256]{1,0:T(2,128)(2,1)S(1)} %slice.45), channel_id=1, source_target_pairs={{0,4},{4,8},{8,12},{12,16},{16,20},{20,24},{24,28},{1,5},{5,9},{9,... | collective-permute-start | bytes 3080 | tf_op jit(solution)/shard_map/ppermute | solution.py:23
  170.2 112.0 %all-to-all-start = ((bf16[4,256,256]{1,2,0:T(8,128)(2,1)}), bf16[4,256,256]{1,2,0:T(8,128)(2,1)S(1)}, u32[]{:S(2)}, u32[]{:S(2)}) async-start(bf16[4,256,256]{1,2,0:T(8,128)(2,1)} %copy.29), calls=%async_computation | async-start | bytes 1048576 | tf_op jit(solution)/shard_map/all_to_all | solution.py:195
  282.3 26.9 %all-to-all-start.2 = ((bf16[8,512,128]{2,1,0:T(8,128)(2,1)}), bf16[8,512,128]{2,1,0:T(8,128)(2,1)S(1)}, u32[]{:S(2)}, u32[]{:S(2)}) async-start(bf16[8,512,128]{2,1,0:T(8,128)(2,1)} %shard_map.131), calls=%async_computation.2 | async-start | bytes 2097152 | tf_op jit(solution)/shard_map/all_to_all | solution.py:199
  312.9 10.9 %all-to-all-start.3 = ((bf16[4,256,256]{1,2,0:T(8,128)(2,1)}), bf16[4,256,256]{1,2,0:T(8,128)(2,1)S(1)}, u32[]{:S(2)}, u32[]{:S(2)}) async-start(bf16[4,256,256]{1,2,0:T(8,128)(2,1)} %copy.39), calls=%async_computation.3 | async-start | bytes 1048576 | tf_op jit(solution)/shard_map/all_to_all | solution.py:204
Sparse Core Ops, SparseCore 0:
  29.5 43.7 all-gather.1
where the time goes:
time: 342 us; the launch traced here: 336 us
  waiting for transfers between devices  120 us (35%)
  Pallas kernels  107 us (31%)
  matrix products  29.5 us (9%)
  starting transfers between devices  24.4 us (7%)
  blocking collectives  22.2 us (6%)
  between operations  14.3 us (4%)
  local copies, waits for them, and re-layouts  10.6 us (3%)
  other arithmetic  8.11 us (2%)
    pallas_call x1, Pallas kernels, attend(): pl.pallas_call(functools.partial(attention_kernel, tok_dev, share, rows,...  107 us
    ppermute x2, waiting for transfers between devices, passed_along(): return lax.ppermute(block, axis, route)  55.9 us
    all_gather x1, waiting for transfers between devices, per_device(): whole_rows = lax.all_gather(tokens, 'tp', axis=1, tiled=True)  39.4 us
    all_gather x1, blocking collectives, per_device(): all_bias = lax.all_gather(break_bias.T, 'sp', axis=1, tiled=True)  22.2 us
    dot_general x5, matrix products, project(): product = jnp.dot(scaled, weight, preferred_element_type=jnp.float32)  19.6 us
    all_to_all x1, waiting for transfers between devices, per_device(): lax.all_to_all(computed, 'sp', split_axis=0, concat_axis=0, tiled=True)  18.4 us
  transfers between devices with their start and end apart: 7, of which 4 were waited for; matrix products, arithmetic and copies ran while one was open for 7% of the time, Pallas kernels for 32%

commit v1 on v0

--- a/solution.py
+++ b/solution.py
@@ -15,6 +15,7 @@
 epsilon = 1e-06
 mass_floor = 0.1
 score_cap = 88.0
+score_cap_fast = 43.0
 
 
 def passed_along(block, axis, distance):
@@ -209,6 +210,700 @@
     return (mixed, mass_logarithm)
 
 
+def tile_core(u):
+    return jnp.where((u == 0) | (u == 3), 0, 1)
+
+
+def tile_at(index, core):
+    return (index // 2) * 4 + jnp.where(index % 2 == 0, core, 3 - core)
+
+
+def scatter_matrix(rows_are_places, n):
+    row = lax.broadcasted_iota(jnp.int32, (n, n), 0)
+    col = lax.broadcasted_iota(jnp.int32, (n, n), 1)
+    place, slot = (row, col) if rows_are_places else (col, row)
+    span = n // 8
+    hit = place == (slot % 8) * span + (span - 1 - slot // 8)
+    return jnp.where(hit, 1.0, 0.0).astype(jnp.bfloat16)
+
+
+def remote(src, dst, send, recv, sp, tp):
+    return pltpu.make_async_remote_copy(
+        src_ref=src,
+        dst_ref=dst,
+        send_sem=send,
+        recv_sem=recv,
+        device_id={"sp": sp, "tp": tp},
+        device_id_type=pl.DeviceIdType.MESH,
+    )
+
+
+def meet(peers):
+    barrier = pltpu.get_barrier_semaphore()
+    for sp, tp in peers:
+        pl.semaphore_signal(
+            barrier, inc=1, device_id={"sp": sp, "tp": tp}, device_id_type=pl.DeviceIdType.MESH
+        )
+    pl.semaphore_wait(barrier, len(peers))
+
+
+def mix_in_kernel(
+    n_sp,
+    heads,
+    tokens,
+    gain,
+    signal_w,
+    post_w,
+    pre_w,
+    query_w,
+    key_w,
+    value_w,
+    taps,
+    bias,
+    gathered,
+    filt,
+    xbuf,
+    scaled,
+    inverse,
+    weights,
+    outgoing,
+    product,
+    rim,
+    rim_out,
+    ready,
+    w_sem,
+    own_sem,
+    ag_send,
+    ag_recv,
+    kv_send,
+    kv_recv,
+    fwd_send,
+    rim_sem,
+    filt_send,
+    filt_recv,
+):
+    p = lax.axis_index("sp")
+    t = lax.axis_index("tp")
+    y, c = t // 2, t % 2
+    mate = 2 * y + 1 - c
+    cross = 2 * (1 - y) + c
+    cross_mate = 2 * (1 - y) + 1 - c
+    tok_dev, shard = tokens.shape
+    n_tp = xbuf.shape[0]
+    size = tok_dev // n_tp
+    width = key_w.shape[1]
+    model = n_tp * shard
+    primary = c == p // heads
+    peers = [((p + k) % n_sp, t) for k in range(1, n_sp)] + [(p, (t + k) % n_tp) for k in range(1, n_tp)]
+
+    sources = (key_w, query_w, value_w, signal_w, pre_w, post_w)
+    loads = [pltpu.make_async_copy(w, weights.at[i], w_sem.at[i]) for i, w in enumerate(sources)]
+    own = [
+        pltpu.make_async_copy(
+            tokens.at[pl.ds(i * size, size)], xbuf.at[t, pl.ds(i * size, size)], own_sem.at[i]
+        )
+        for i in range(n_tp)
+    ]
+    own[0].start()
+    for load in loads[:3]:
+        load.start()
+    meet(peers)
+
+    def token_copy(kind, i):
+        rows = pl.ds(i * size, size)
+        if kind == 0:
+            return remote(tokens.at[rows], xbuf.at[t, rows], ag_send.at[0, i], ag_recv.at[0, i], p, cross)
+        if kind == 1:
+            return remote(tokens.at[rows], xbuf.at[t, rows], ag_send.at[1, i], ag_recv.at[1, i], p, mate)
+        return remote(
+            xbuf.at[cross, rows], xbuf.at[cross, rows], ag_send.at[2, i], ag_recv.at[2, i], p, mate
+        )
+
+    for i in range(n_tp):
+        token_copy(0, i).start()
+    for i in range(n_tp):
+        token_copy(1, i).start()
+    for copy in own[1:]:
+        copy.start()
+    for load in loads[3:]:
+        load.start()
+    for load in loads[:3]:
+        load.wait()
+    order = scatter_matrix(False, size)
+    lane = lax.broadcasted_iota(jnp.int32, (size, 128), 1)
+    step = 32
+
+    def kv_copy(i, h):
+        target = c * heads + h
+        stays = target == p
+        sp = jnp.where(stays, p, target)
+        tp = jnp.where(stays, mate, t)
+        return remote(
+            outgoing.at[i, h], gathered.at[p, i], kv_send.at[i, h], kv_recv.at[p, i], sp, tp
+        )
+
+    @pl.loop(0, n_tp)
+    def _(i):
+        rows = pl.ds(pl.multiple_of(i * size, size), size)
+        pltpu.make_async_copy(tokens.at[rows], xbuf.at[t, rows], own_sem.at[i]).wait()
+        token_copy(0, i).wait_recv()
+        token_copy(2, i).start()
+        token_copy(1, i).wait_recv()
+        token_copy(2, i).wait_recv()
+
+        @pl.loop(0, size // step)
+        def _(k):
+            place = pl.ds(pl.multiple_of(i * size + k * step, step), step)
+            total = jnp.zeros((step, 1), jnp.float32)
+            for part in range(n_tp):
+                x = xbuf[part, place, :].astype(jnp.float32)
+                total = total + jnp.sum(x * x, axis=1, keepdims=True)
+                columns = slice(part * shard, (part + 1) * shard)
+                scaled[place, columns] = (x * gain[:, columns]).astype(jnp.bfloat16)
+            inverse[place, :] = lax.rsqrt(total * (1.0 / model) + epsilon)
+
+        x = scaled[rows, :]
+        inv = inverse[rows, :]
+
+        def project(index):
+            y_ = jnp.dot(x, weights[index], preferred_element_type=jnp.float32)
+            return (y_ * inv).astype(jnp.bfloat16)
+
+        k_rows = jnp.dot(order, project(0), preferred_element_type=jnp.float32)
+        q_rows = jnp.dot(order, project(1), preferred_element_type=jnp.float32) * (HEAD_DIM**-0.5)
+        v_cols = jnp.dot(order, project(2), preferred_element_type=jnp.float32).T
+        bias_rows = jnp.dot(order, bias[rows, :], preferred_element_type=jnp.float32)
+        bias_rows = jnp.concatenate(
+            [bias_rows, jnp.zeros((size, 128 - heads), jnp.float32)], axis=1
+        ).T
+        half = 2 * HEAD_DIM
+        for h in range(heads):
+            pair = slice((h // 2) * half, (h // 2 + 1) * half)
+            kp, qp = k_rows[:, pair], q_rows[:, pair]
+            if h % 2 == 0:
+                kq = jnp.where(lane < HEAD_DIM, kp, pltpu.roll(qp, HEAD_DIM, 1))
+            else:
+                kq = jnp.where(lane < HEAD_DIM, pltpu.roll(kp, HEAD_DIM, 1), qp)
+            kq = kq.astype(jnp.bfloat16)
+            first = lax.broadcasted_iota(jnp.int32, (16, size), 0) == 0
+            tail = jnp.where(first, bias_rows[h : h + 1, :], 0.0)
+            vb = jnp.concatenate([v_cols[h * HEAD_DIM : (h + 1) * HEAD_DIM, :], tail], axis=0)
+            vb = vb.astype(jnp.bfloat16)
+            deep = HEAD_DIM + 16
+
+            def put(ref):
+                ref[0:size, :] = kq
+                ref[size : size + deep, :] = vb[:, :128]
+                ref[size + deep : size + 2 * deep, :] = vb[:, 128:]
+
+            put(outgoing.at[i, h])
+
+            @pl.when(c * heads + h == p)
+            def _():
+                put(gathered.at[p, i])
+
+            kv_copy(i, h).start()
+
+    for load in loads[3:]:
+        load.wait()
+
+    def gate(u):
+        rows = pl.ds(u * size, size)
+        x = scaled[rows, :]
+        inv = inverse[rows, :]
+        outs = []
+        for index in range(3, 6):
+            y_ = jnp.dot(x, weights[index], preferred_element_type=jnp.float32)
+            outs.append((y_ * inv).astype(jnp.bfloat16))
+        product[pl.ds(8 + u * size, size), :] = outs[1].astype(jnp.float32) * outs[0].astype(jnp.float32)
+        ready[rows, :] = outs[2]
+
+    gate(n_tp - 1)
+    rim_out[...] = product[pl.ds(tok_dev, 8), :]
+    rim_copy = remote(rim_out, rim, rim_sem.at[0], rim_sem.at[1], (p + 1) % n_sp, t)
+    rim_copy.start()
+    for u in range(n_tp - 1):
+        gate(u)
+    rim_copy.wait()
+    product[0:8, :] = jnp.where(p > 0, rim[...], 0.0)
+    tap_values = taps[...].astype(jnp.float32)
+
+    def filt_copy(u):
+        return remote(ready.at[pl.ds(u * size, size)], filt.at[t], filt_send.at[u], filt_recv.at[t], p, u)
+
+    for u in range(n_tp):
+        running = jnp.zeros((size, width), jnp.float32)
+        for w in range(CONV_W):
+            start = 8 - (CONV_W - 1) + w + u * size
+            running = running + tap_values[w : w + 1, :] * product[pl.ds(start, size), :]
+        rows = pl.ds(u * size, size)
+        done = (ready[rows, :].astype(jnp.float32) * running).astype(jnp.bfloat16)
+        ready[rows, :] = done
+
+        @pl.when(t == u)
+        def _():
+            filt[u] = done
+
+        @pl.when(t != u)
+        def _():
+            filt_copy(u).start()
+
+    def arrival(b, i):
+        return remote(outgoing.at[i, 0], gathered.at[b, i], fwd_send.at[b, i], kv_recv.at[b, i], p, mate)
+
+    def forward(b, i):
+        return remote(gathered.at[b, i], gathered.at[b, i], fwd_send.at[b, i], kv_recv.at[b, i], p, mate)
+
+    @pl.when(primary)
+    def _():
+        @pl.loop(0, n_tp)
+        def _(i):
+            @pl.loop(1, n_sp)
+            def _(k):
+                b = (p + k) % n_sp
+                arrival(b, i).wait_recv()
+                forward(b, i).start()
+
+        @pl.loop(0, n_tp)
+        def _(i):
+            @pl.loop(1, n_sp)
+            def _(k):
+                forward((p + k) % n_sp, i).wait_send()
+
+    @pl.when(jnp.logical_not(primary))
+    def _():
+        @pl.loop(0, n_tp)
+        def _(i):
+            @pl.loop(0, n_sp)
+            def _(b):
+                arrival(b, i).wait_recv()
+
+    for i in range(n_tp):
+        for kind in range(3):
+            token_copy(kind, i).wait_send()
+        for h in range(heads):
+            kv_copy(i, h).wait_send()
+    for k in range(1, n_tp):
+        u = (t + k) % n_tp
+        remote(ready.at[pl.ds(0, size)], filt.at[u], filt_send.at[u], filt_recv.at[u], p, u).wait()
+
+
+def mix_in(tokens, norm_gain, projections, taps, bias, n_sp, n_tp):
+    tok_dev, shard = tokens.shape
+    heads = bias.shape[1]
+    width = projections[0].shape[1]
+    model = n_tp * shard
+    size = tok_dev // n_tp
+    block = size + 2 * (HEAD_DIM + 16)
+    vmem = pl.BlockSpec(memory_space=pltpu.VMEM)
+    anywhere = pl.BlockSpec(memory_space=pl.ANY)
+    dma = pltpu.SemaphoreType.DMA
+    bf16, f32 = jnp.bfloat16, jnp.float32
+    signal_w, post_w, pre_w, query_w, key_w, value_w = projections
+    return pl.pallas_call(
+        functools.partial(mix_in_kernel, n_sp, heads),
+        out_shape=[
+            jax.ShapeDtypeStruct((n_sp, n_tp, block, 128), bf16),
+            jax.ShapeDtypeStruct((n_tp, size, width), bf16),
+        ],
+        in_specs=[anywhere, vmem] + [anywhere] * 6 + [vmem, vmem],
+        out_specs=[vmem, vmem],
+        scratch_shapes=[
+            pltpu.VMEM((n_tp, tok_dev, shard), bf16),
+            pltpu.VMEM((tok_dev, model), bf16),
+            pltpu.VMEM((tok_dev, 1), f32),
+            pltpu.VMEM((6, model, width), bf16),
+            pltpu.VMEM((n_tp, heads, block, 128), bf16),
+            pltpu.VMEM((tok_dev + 8, width), f32),
+            pltpu.VMEM((8, width), f32),
+            pltpu.VMEM((8, width), f32),
+            pltpu.VMEM((tok_dev, width), bf16),
+            dma((6,)),
+            dma((n_tp,)),
+            dma((3, n_tp)),
+            dma((3, n_tp)),
+            dma((n_tp, heads)),
+            dma((n_sp, n_tp)),
+            dma((n_sp, n_tp)),
+            dma((2,)),
+            dma((n_tp,)),
+            dma((n_tp,)),
+        ],
+        compiler_params=pltpu.CompilerParams(
+            collective_id=0, has_side_effects=True, vmem_limit_bytes=60 * 1024 * 1024
+        ),
+        name="mix_in",
+    )(tokens, norm_gain.reshape(1, model), signal_w, post_w, pre_w, query_w, key_w, value_w, taps, bias)
+
+
+def later_product(total):
+    n = total.shape[0]
+    row = lax.broadcasted_iota(jnp.int32, total.shape, 0)
+    x = jnp.where(row < n - 1, pltpu.roll(total, n - 1, 0), 1.0)
+    k = 1
+    while k < n:
+        x = x * jnp.where(row < n - k, pltpu.roll(x, n - k, 0), 1.0)
+        k *= 2
+    return x
+
+
+def stick_kernel(got, out, mass, keys, quer, acc, carry, w0, w1, r0, r1):
+    p = lax.axis_index("sp")
+    core = lax.axis_index("tp") % 2
+    n_sp, subs = got.shape[:2]
+    size = quer.shape[1]
+    deep = HEAD_DIM + 16
+    n_tiles = quer.shape[0]
+    groups = size // 8
+    wb, rb = (w0, w1), (r0, r1)
+    lane = lax.broadcasted_iota(jnp.int32, (size, 128), 1)
+    unit = (lax.broadcasted_iota(jnp.int32, (16, 128), 0) == 0) & (
+        lax.broadcasted_iota(jnp.int32, (16, 128), 1) == HEAD_DIM
+    )
+    unit = jnp.where(unit, 1.0, 0.0).astype(jnp.bfloat16)
+    constant = jnp.where(lane == HEAD_DIM, 1.0, 0.0)
+
+    @pl.loop(0, n_sp)
+    def _(b):
+        for i in range(subs):
+            kq = got[b, i, 0:size, :]
+            tail = jnp.concatenate(
+                [
+                    got[b, i, size + HEAD_DIM : size + deep, :],
+                    got[b, i, size + deep + HEAD_DIM : size + 2 * deep, :],
+                ],
+                axis=1,
+            )
+            column = lax.dot_general(
+                tail, unit, (((0,), (0,)), ((), ())), preferred_element_type=jnp.float32
+            )
+            keys[b, i] = jnp.where(lane < HEAD_DIM, kq.astype(jnp.float32), column).astype(jnp.bfloat16)
+
+    @pl.loop(0, n_tiles)
+    def _(index):
+        tile = tile_at(index, core)
+        rolled = pltpu.roll(got[tile // subs, tile % subs, 0:size, :].astype(jnp.float32), HEAD_DIM, 1)
+        quer[index] = jnp.where(lane < HEAD_DIM, rolled, constant).astype(jnp.bfloat16)
+
+    col = lax.broadcasted_iota(jnp.int32, (8, size), 1)
+    place = (col % 8) * groups + (groups - 1) - col // 8
+    segment = lax.broadcasted_iota(jnp.int32, (8, size), 0) * groups
+    relative = place - segment
+
+    def early(slot, index, b, masked):
+        q = quer[index]
+        tile = tile_at(index, core)
+        for s in range(subs):
+            scores = lax.dot_general(
+                keys[b, s], q, (((1,), (1,)), ((), ())), preferred_element_type=jnp.float32
+            )
+            shift = (tile % subs - s) * size
+            run = None
+            for j in range(groups):
+                e = jnp.exp(jnp.minimum(scores[8 * j : 8 * j + 8, :], score_cap_fast))
+                if masked:
+                    e = jnp.where(relative + shift > groups - 1 - j, e, 0.0)
+                r = 1.0 / (1.0 + e)
+                run = r if run is None else run * r
+                w = e * run
+                if j % 2:
+                    pair = jnp.concatenate([before, w], axis=0).astype(jnp.bfloat16)
+                    wb[slot][s, 8 * (j - 1) : 8 * (j + 1), :] = pair
+                before = w
+            rb[slot][s] = run
+
+    def late(slot, index, b):
+        first = b == tile_at(index, core) // subs
+        running = jnp.where(first, 1.0, carry[...])
+        total = jnp.where(first, 0.0, acc[...])
+        for s in range(subs - 1, -1, -1):
+            run = rb[slot][s]
+            factor = later_product(run) * running
+            running = jnp.broadcast_to((factor * run)[:1], run.shape)
+            twice = jnp.concatenate([factor, factor], axis=0).astype(jnp.bfloat16)
+            pieces = [wb[slot][s, 16 * j : 16 * j + 16, :] * twice for j in range(groups // 2)]
+            values = jnp.concatenate(
+                [got[b, s, size : size + HEAD_DIM, :], got[b, s, size + deep : size + deep + HEAD_DIM, :]],
+                axis=1,
+            )
+            total = total + jnp.dot(
+                values, jnp.concatenate(pieces, axis=0), preferred_element_type=jnp.float32
+            )
+        acc[...] = total
+        carry[...] = running
+        out[index] = total.astype(jnp.bfloat16)
+        mass[index] = jnp.log(jnp.maximum(1.0 - running, mass_floor))
+
+    def block_of(index):
+        return tile_at(index, core) // subs
+
+    items = 0
+    for index in range(n_tiles):
+        items = items + (index // 2) + 1
+    steps = items + 1
+    skip = steps % 2
+
+    def half(z, m, state):
+        i1, b1, i2, b2 = state
+
+        def go(masked):
+            late(z, i2, b2)
+            early(1 - z, i1, b1, masked)
+
+        lax.cond(b1 == block_of(i1), lambda: go(True), lambda: go(False))
+        last = b1 == 0
+        after = jnp.minimum(i1 + 1, n_tiles - 1)
+        ni = jnp.where(last, after, i1)
+        nb = jnp.where(last, block_of(after), b1 - 1)
+        advance = m >= 0
+        return jnp.where(advance, ni, i1), jnp.where(advance, nb, b1), i1, b1
+
+    def body(k, state):
+        for z in range(2):
+            state = half(z, 2 * k + z - skip, state)
+        return state
+
+    zero = jnp.int32(0)
+    lax.fori_loop(0, (steps + skip) // 2, body, (zero, zero, zero, zero))
+
+
+def stick(gathered):
+    n_sp, subs, block, _ = gathered.shape
+    size = block - 2 * (HEAD_DIM + 16)
+    n_tiles = n_sp * subs // 2
+    vmem = pl.BlockSpec(memory_space=pltpu.VMEM)
+    bf16, f32 = jnp.bfloat16, jnp.float32
+    pairs = n_tiles * size * (n_sp + 1) * subs * size // 2
+    return pl.pallas_call(
+        stick_kernel,
+        out_shape=[
+            jax.ShapeDtypeStruct((n_tiles, HEAD_DIM, size), bf16),
+            jax.ShapeDtypeStruct((n_tiles, 8, size), f32),
+        ],
+        in_specs=[vmem],
+        out_specs=[vmem, vmem],
+        scratch_shapes=[
+            pltpu.VMEM((n_sp, subs, size, 128), bf16),
+            pltpu.VMEM((n_tiles, size, 128), bf16),
+            pltpu.VMEM((HEAD_DIM, size), f32),
+            pltpu.VMEM((8, size), f32),
+            pltpu.VMEM((subs, size, size), bf16),
+            pltpu.VMEM((subs, size, size), bf16),
+            pltpu.VMEM((subs, 8, size), f32),
+            pltpu.VMEM((subs, 8, size), f32),
+        ],
+        compiler_params=pltpu.CompilerParams(vmem_limit_bytes=48 * 1024 * 1024),
+        cost_estimate=pl.CostEstimate(
+            flops=pairs * 4 * HEAD_DIM, bytes_accessed=gathered.size * 2, transcendentals=2 * pairs
+        ),
+        name="stick",
+    )(gathered)
+
+
+def mix_out_kernel(
+    n_sp,
+    heads,
+    tiles,
+    mass,
+    filt,
+    filter_w,
+    attend_w,
+    mixed,
+    logs,
+    arrived,
+    marks,
+    wf,
+    wa,
+    partial,
+    attended,
+    w_sem,
+    a_send,
+    a_recv,
+    m_send,
+    m_recv,
+):
+    p = lax.axis_index("sp")
+    t = lax.axis_index("tp")
+    y, c = t // 2, t % 2
+    n_tp, size, width = filt.shape
+    n_tiles = tiles.shape[0]
+    owner = 2 * y + p // heads
+    head = owner * heads + p % heads
+    total_heads = arrived.shape[0]
+    loads = [
+        pltpu.make_async_copy(filter_w, wf, w_sem.at[0]),
+        pltpu.make_async_copy(attend_w, wa, w_sem.at[1]),
+    ]
+    for load in loads:
+        load.start()
+    peers = []
+    for a in range(n_sp):
+        for b in range(n_tp):
+            if a or b:
+                peers.append(((p + a) % n_sp, (t + b) % n_tp))
+    meet(peers)
+
+    def tile_copy(index):
+        tile = tile_at(index, c)
+        b, u = tile // n_tp, tile % n_tp
+        return remote(tiles.at[index], arrived.at[head], a_send.at[index], a_recv.at[head], b, u)
+
+    def mark_copy(index):
+        tile = tile_at(index, c)
+        b, u = tile // n_tp, tile % n_tp
+        slot = p % heads * n_tp + u
+        return remote(mass.at[index], marks.at[slot], m_send.at[index], m_recv.at[slot], b, owner)
+
+    def each(index, act):
+        tile = tile_at(index, c)
+        b, u = tile // n_tp, tile % n_tp
+        own_tile = (b == p) & (u == t)
+        own_mark = (b == p) & (owner == t)
+        if act == "start":
+
+            @pl.when(own_tile)
+            def _():
+                arrived[head] = tiles[index]
+
+            @pl.when(own_mark)
+            def _():
+                marks[p % heads * n_tp + u] = mass[index]
+
+        @pl.when(jnp.logical_not(own_tile))
+        def _():
+            copy = tile_copy(index)
+            copy.start() if act == "start" else copy.wait_send()
+
+        @pl.when(jnp.logical_not(own_mark))
+        def _():
+            copy = mark_copy(index)
+            copy.start() if act == "start" else copy.wait_send()
+
+    pl.loop(0, n_tiles)(lambda index: each(index, "start"))
+    loads[0].wait()
+    columns = 256
+
+    @pl.loop(0, mixed.shape[1] // columns)
+    def _(k):
+        at = pl.ds(pl.multiple_of(k * columns, columns), columns)
+        total = jnp.zeros((size, columns), jnp.float32)
+        for part in range(n_tp):
+            total = total + jnp.dot(
+                filt[part], wf[part * width : (part + 1) * width, at], preferred_element_type=jnp.float32
+            )
+        partial[:, at] = total
+
+    loads[1].wait()
+    mine = tile_core(t) == c
+
+    @pl.loop(0, total_heads)
+    def _(k):
+        @pl.when(jnp.logical_not((k == head) & mine))
+        def _():
+            remote(tiles.at[0], arrived.at[k], a_send.at[0], a_recv.at[k], p, t).wait_recv()
+
+    order = scatter_matrix(True, size)
+    for part in range(n_tp):
+        stack = jnp.concatenate([arrived[part * heads + h] for h in range(heads)], axis=0)
+        rows = lax.dot_general(order, stack, (((1,), (1,)), ((), ())), preferred_element_type=jnp.float32)
+        attended[:, part * width : (part + 1) * width] = rows.astype(jnp.bfloat16)
+
+    @pl.loop(0, mixed.shape[1] // columns)
+    def _(k):
+        at = pl.ds(pl.multiple_of(k * columns, columns), columns)
+        total = partial[:, at] + jnp.dot(attended[...], wa[:, at], preferred_element_type=jnp.float32)
+        mixed[:, at] = total.astype(jnp.bfloat16)
+
+    @pl.loop(0, heads)
+    def _(h):
+        for u in range(n_tp):
+            own = (p == c * heads + h) & (tile_core(u) == c)
+
+            @pl.when(jnp.logical_not(own))
+            def _():
+                slot = h * n_tp + u
+                remote(mass.at[0], marks.at[slot], m_send.at[0], m_recv.at[slot], p, t).wait_recv()
+
+    back = scatter_matrix(False, size)
+    for u in range(n_tp):
+        row = lax.broadcasted_iota(jnp.int32, (8, size), 0)
+        value = jnp.zeros((8, size), jnp.float32)
+        for h in range(heads):
+            value = jnp.where(row == h, marks[h * n_tp + u], value)
+        total = jnp.zeros((8, size), jnp.float32)
+        for _ in range(3):
+            high = value.astype(jnp.bfloat16)
+            value = value - high.astype(jnp.float32)
+            total = total + jnp.dot(high, back, preferred_element_type=jnp.float32)
+        logs[:, u * size : (u + 1) * size] = total[:heads]
+    pl.loop(0, n_tiles)(lambda index: each(index, "wait"))
+
+
+def mix_out(tiles, mass, filt, filter_readout, attention_readout, n_sp, heads):
+    n_tp, size, width = filt.shape
+    model = filter_readout.shape[1]
+    vmem = pl.BlockSpec(memory_space=pltpu.VMEM)
+    anywhere = pl.BlockSpec(memory_space=pl.ANY)
+    dma = pltpu.SemaphoreType.DMA
+    bf16, f32 = jnp.bfloat16, jnp.float32
+    n_tiles = tiles.shape[0]
+    return pl.pallas_call(
+        functools.partial(mix_out_kernel, n_sp, heads),
+        out_shape=[
+            jax.ShapeDtypeStruct((size, model), bf16),
+            jax.ShapeDtypeStruct((heads, n_tp * size), f32),
+        ],
+        in_specs=[vmem, vmem, vmem, anywhere, anywhere],
+        out_specs=[vmem, vmem],
+        scratch_shapes=[
+            pltpu.VMEM((heads * n_tp, HEAD_DIM, size), bf16),
+            pltpu.VMEM((heads * n_tp, 8, size), f32),
+            pltpu.VMEM(filter_readout.shape, bf16),
+            pltpu.VMEM(attention_readout.shape, bf16),
+            pltpu.VMEM((size, model), f32),
+            pltpu.VMEM((size, n_tp * width), bf16),
+            dma((2,)),
+            dma((n_tiles,)),
+            dma((heads * n_tp,)),
+            dma((n_tiles,)),
+            dma((heads * n_tp,)),
+        ],
+        compiler_params=pltpu.CompilerParams(
+            collective_id=1, has_side_effects=True, vmem_limit_bytes=60 * 1024 * 1024
+        ),
+        name="mix_out",
+    )(tiles, mass, filt, filter_readout, attention_readout)
+
+
+def per_device_fast(
+    tokens,
+    norm_gain,
+    signal_proj,
+    postgate_proj,
+    pregate_proj,
+    query_proj,
+    key_proj,
+    value_proj,
+    filter_taps,
+    break_bias,
+    filter_readout,
+    attention_readout,
+):
+    n_sp, n_tp = lax.axis_size("sp"), lax.axis_size("tp")
+    projections = (signal_proj, postgate_proj, pregate_proj, query_proj, key_proj, value_proj)
+    gathered, filt = mix_in(tokens, norm_gain, projections, filter_taps, break_bias, n_sp, n_tp)
+    tiles, mass = stick(gathered)
+    return mix_out(tiles, mass, filt, filter_readout, attention_readout, n_sp, break_bias.shape[1])
+
+
+def per_device_any(*operands):
+    tok_dev = operands[0].shape[0]
+    heads_dev = operands[9].shape[1]
+    n_sp, n_tp = lax.axis_size("sp"), lax.axis_size("tp")
+    fast = n_tp == 4 and n_sp == 2 * heads_dev and tok_dev == n_tp * 256 and operands[6].shape[1] == 256
+    return (per_device_fast if fast else per_device)(*operands)
+
+
 def solution(mesh):
     placed = (
         P("sp", "tp"),
@@ -225,7 +920,7 @@
         P(),
     )
     return jax.shard_map(
-        per_device,
+        per_device_any,
         mesh=mesh,
         in_specs=placed,
         out_specs=(P(("sp", "tp"), None), P("tp", "sp")),

time: 342 us -> 140 us (0.41); the launches traced: 336 us -> 140 us
  waiting for transfers between devices: 120 us -> 0 us
  matrix products: 29.5 us -> 0 us
  starting transfers between devices: 24.4 us -> 0 us
  Pallas kernels: 107 us -> 130 us
  blocking collectives: 22.2 us -> 0 us
  between operations: 14.3 us -> 0.67 us
  other arithmetic: 8.11 us -> 0 us
    ppermute x2 -> x0, waiting for transfers between devices: 55.9 us -> none  [passed_along(): return lax.ppermute(block, axis, route)]
    all_gather x1 -> x0, waiting for transfers between devices: 39.4 us -> none  [per_device(): whole_rows = lax.all_gather(tokens, 'tp', axis=1, tiled=True)]
    dot_general x7 -> x0, matrix products: 29.5 us -> none  [the longest x5 19.6 us: project(): product = jnp.dot(scaled, weight, preferred_element_type=jnp.float32)]
    all_to_all x4 -> x0, waiting for transfers between devices: 24.4 us -> none  [the longest x1 18.4 us: per_device(): lax.all_to_all(computed, 'sp', split_axis=0, concat_axis=0, tiled=True)]
    pallas_call x1 -> x3, Pallas kernels: 107 us -> 130 us  [the longest x1 62.5 us: mix_in(): pl.pallas_call(functools.partial(mix_in_kernel, n_sp, heads), out_shape=[...]
    all_gather x1 -> x0, blocking collectives: 22.2 us -> none  [per_device(): all_bias = lax.all_gather(break_bias.T, 'sp', axis=1, tiled=True)]
    all_to_all x4 -> x0, starting transfers between devices: 18.2 us -> none  [the longest x1 5.61 us: per_device(): lax.all_to_all(outgoing, 'sp', split_axis=0, concat_axis=0, tiled=True)]
    ppermute x2 -> x0, starting transfers between devices: 6.17 us -> none  [passed_along(): return lax.ppermute(block, axis, route)]
  transfers between devices with their start and end apart: 7 -> 0, of which waited for: 4 -> 0; matrix products, arithmetic and copies ran while one was open for 7% -> 0% of each run, Pallas kernels for 32% -> 0%
where the time goes in v1:
time: 140 us
  Pallas kernels  130 us (93%)
  local copies, waits for them, and re-layouts  8.59 us (6%)
    pallas_call x1, Pallas kernels, mix_in(): pl.pallas_call(functools.partial(mix_in_kernel, n_sp, heads), out_shape=[...  62.5 us
    pallas_call x1, Pallas kernels, stick(): pl.pallas_call(stick_kernel, out_shape=[jax.ShapeDtypeStruct((n_tiles, HE...  41.7 us
    pallas_call x1, Pallas kernels, mix_out(): pl.pallas_call(functools.partial(mix_out_kernel, n_sp, heads), out_shape=...  26.2 us
    unnamed x9, local copies, waits for them, and re-layouts  8.59 us

profile of v1, /device:TPU:15, one launch (start us, length us, event | category | flops | bytes accessed | tf_op | source)
XLA Modules:
  0.0 139.7 jit_solution(743976584380178061)
XLA Ops:
  0.6 1.6 %copy.14.bias = bf16[1024,4]{1,0:T(8,128)(2,1)} copy(bf16[1024,4]{0,1:T(4,128)(2,1)} %param.21) | data formatting | bytes 16384 | tf_op args[9]
  2.2 62.5 %mix_in.1 = (bf16[8,4,416,128]{3,2,1,0:T(8,128)(2,1)}, bf16[4,256,256]{2,1,0:T(8,128)(2,1)}) custom-call(bf16[1024,512]{1,0:T(8,128)(2,1)} %tokens.1, f32[1,2048]{1,0:T(1,128)} %bitcast.1, bf16[2048,256]{1,0:T(8,128)(2,1)} %signal_w.1, bf16[2048,256]{1,0:T(8,128)(2,1)} %post_w.1, bf16[2048,256]{1,0:T(8,128)(2,1)} %pre_w.1, bf16[2048,256]{1,0:T(8,128)(2,1)} %query_w.1, ...), custom_call_target="tpu_custom_call" | custom-call | tf_op jit(solution)/shard_map/mix_in/pallas_call | solution.py:503
  64.8 0.0 copy-start.2
  64.8 2.0 %copy-done.2 = bf16[8,4,416,128]{3,2,1,0:T(8,128)(2,1)S(1)} copy-done((bf16[8,4,416,128]{3,2,1,0:T(8,128)(2,1)S(1)}, bf16[8,4,416,128]{3,2,1,0:T(8,128)(2,1)}, u32[]{:S(2)}) %copy-start.2) | copy-done | bytes 3407896
  66.7 41.7 %stick.1 = (bf16[16,64,256]{2,1,0:T(8,128)(2,1)S(1)}, f32[16,8,256]{2,1,0:T(8,128)S(1)}) custom-call(bf16[8,4,416,128]{3,2,1,0:T(8,128)(2,1)S(1)} %copy-done.2), custom_call_target="tpu_custom_call" | custom-call | flops 4831838208 | bytes 3407872 | tf_op jit(solution)/shard_map/stick/pallas_call | solution.py:677
  108.5 0.0 copy-start
  108.5 0.8 copy-done
  109.3 0.0 copy-start.1
  109.3 0.6 copy-done.1
  109.9 26.2 %mix_out.1 = (bf16[256,2048]{1,0:T(8,128)(2,1)}, f32[4,1024]{1,0:T(4,128)}) custom-call(bf16[16,64,256]{2,1,0:T(8,128)(2,1)} %copy-done, f32[16,8,256]{2,1,0:T(8,128)} %copy-done.1, bf16[4,256,256]{2,1,0:T(8,128)(2,1)} %get-tuple-element.9.filt, bf16[1024,2048]{1,0:T(8,128)(2,1)} %filter_w.1, bf16[1024,2048]{1,0:T(8,128)(2,1)} %attend_w.1), custom_call_target="tpu_custom_call" | custom-call | tf_op jit(solution)/shard_map/mix_out/pallas_call | solution.py:850
  136.1 2.3 %copy.17 = bf16[256,2048]{1,0:T(8,128)(2,1)} copy(bf16[256,2048]{1,0:T(8,128)(2,1)} %get-tuple-element.12) | data formatting | bytes 2097152
  138.4 1.3 copy.18
Async XLA Ops:
  64.8 2.0 %copy-start.2 = (bf16[8,4,416,128]{3,2,1,0:T(8,128)(2,1)S(1)}, bf16[8,4,416,128]{3,2,1,0:T(8,128)(2,1)}, u32[]{:S(2)}) copy-start(bf16[8,4,416,128]{3,2,1,0:T(8,128)(2,1)} %get-tuple-element.6.got) | copy-start | bytes 10223620
  108.5 0.8 copy-start
  109.3 0.6 copy-start.1

commit v2 on v0

--- a/solution.py
+++ b/solution.py
@@ -15,6 +15,7 @@
 epsilon = 1e-06
 mass_floor = 0.1
 score_cap = 88.0
+score_cap_fast = 43.0
 
 
 def passed_along(block, axis, distance):
@@ -209,6 +210,690 @@
     return (mixed, mass_logarithm)
 
 
+def tile_core(u):
+    return jnp.where((u == 0) | (u == 3), 0, 1)
+
+
+def tile_at(index, core):
+    return (index // 2) * 4 + jnp.where(index % 2 == 0, core, 3 - core)
+
+
+def scatter_matrix(rows_are_places, n):
+    row = lax.broadcasted_iota(jnp.int32, (n, n), 0)
+    col = lax.broadcasted_iota(jnp.int32, (n, n), 1)
+    place, slot = (row, col) if rows_are_places else (col, row)
+    span = n // 8
+    hit = place == (slot % 8) * span + (span - 1 - slot // 8)
+    return jnp.where(hit, 1.0, 0.0).astype(jnp.bfloat16)
+
+
+def remote(src, dst, send, recv, sp, tp):
+    return pltpu.make_async_remote_copy(
+        src_ref=src,
+        dst_ref=dst,
+        send_sem=send,
+        recv_sem=recv,
+        device_id={"sp": sp, "tp": tp},
+        device_id_type=pl.DeviceIdType.MESH,
+    )
+
+
+def meet(peers):
+    barrier = pltpu.get_barrier_semaphore()
+    for sp, tp in peers:
+        pl.semaphore_signal(
+            barrier, inc=1, device_id={"sp": sp, "tp": tp}, device_id_type=pl.DeviceIdType.MESH
+        )
+    pl.semaphore_wait(barrier, len(peers))
+
+
+def later_product(total):
+    n = total.shape[0]
+    row = lax.broadcasted_iota(jnp.int32, total.shape, 0)
+    x = jnp.where(row < n - 1, pltpu.roll(total, n - 1, 0), 1.0)
+    k = 1
+    while k < n:
+        x = x * jnp.where(row < n - k, pltpu.roll(x, n - k, 0), 1.0)
+        k *= 2
+    return x
+
+
+def layer_kernel(
+    n_sp,
+    heads,
+    tokens,
+    gain,
+    signal_w,
+    post_w,
+    pre_w,
+    query_w,
+    key_w,
+    value_w,
+    taps,
+    bias,
+    filter_w,
+    attend_w,
+    mixed,
+    logs,
+    xbuf,
+    scaled,
+    inverse,
+    weights,
+    outgoing,
+    gathered,
+    product,
+    rim,
+    rim_out,
+    ready,
+    filt,
+    keys,
+    quer,
+    acc,
+    carry,
+    w0,
+    w1,
+    r0,
+    r1,
+    tiles,
+    mass,
+    arrived,
+    marks,
+    wf,
+    wa,
+    partial,
+    attended,
+    w_sem,
+    own_sem,
+    ag_send,
+    ag_recv,
+    kv_send,
+    kv_recv,
+    fwd_send,
+    rim_sem,
+    filt_send,
+    filt_recv,
+    a_send,
+    a_recv,
+    m_send,
+    m_recv,
+):
+    p = lax.axis_index("sp")
+    t = lax.axis_index("tp")
+    y, c = t // 2, t % 2
+    mate = 2 * y + 1 - c
+    cross = 2 * (1 - y) + c
+    tok_dev, shard = tokens.shape
+    n_tp = xbuf.shape[0]
+    size = tok_dev // n_tp
+    width = key_w.shape[1]
+    model = n_tp * shard
+    half_sp = n_sp // 2
+    upper = p // half_sp
+    primary = c == p // heads
+    owner = 2 * y + p // heads
+    head = owner * heads + p % heads
+    total_heads = arrived.shape[0]
+    n_tiles = tiles.shape[0]
+    groups = size // 8
+
+    sources = (key_w, query_w, value_w, signal_w, pre_w, post_w)
+    loads = [pltpu.make_async_copy(w, weights.at[i], w_sem.at[i]) for i, w in enumerate(sources)]
+    loads.append(pltpu.make_async_copy(filter_w, wf, w_sem.at[6]))
+    loads.append(pltpu.make_async_copy(attend_w, wa, w_sem.at[7]))
+    own = [
+        pltpu.make_async_copy(
+            tokens.at[pl.ds(i * size, size)], xbuf.at[t, pl.ds(i * size, size)], own_sem.at[i]
+        )
+        for i in range(n_tp)
+    ]
+    own[0].start()
+    for load in loads[:3]:
+        load.start()
+    peers = []
+    for a in range(n_sp):
+        for b in range(n_tp):
+            if a or b:
+                peers.append(((p + a) % n_sp, (t + b) % n_tp))
+    meet(peers)
+
+    def token_copy(kind, i):
+        rows = pl.ds(i * size, size)
+        if kind == 0:
+            return remote(tokens.at[rows], xbuf.at[t, rows], ag_send.at[0, i], ag_recv.at[0, i], p, cross)
+        if kind == 1:
+            return remote(tokens.at[rows], xbuf.at[t, rows], ag_send.at[1, i], ag_recv.at[1, i], p, mate)
+        return remote(
+            xbuf.at[cross, rows], xbuf.at[cross, rows], ag_send.at[2, i], ag_recv.at[2, i], p, mate
+        )
+
+    for i in range(n_tp):
+        token_copy(0, i).start()
+    for i in range(n_tp):
+        token_copy(1, i).start()
+    for copy in own[1:]:
+        copy.start()
+    for load in loads[3:]:
+        load.start()
+    for load in loads[:3]:
+        load.wait()
+    order = scatter_matrix(False, size)
+    back = scatter_matrix(True, size)
+    lane = lax.broadcasted_iota(jnp.int32, (size, 128), 1)
+    step = 32
+
+    def kv_copy(i, h):
+        target = c * heads + h
+        stays = target == p
+        sp = jnp.where(stays, p, target)
+        tp = jnp.where(stays, mate, t)
+        return remote(
+            outgoing.at[i, h], gathered.at[p, i], kv_send.at[i, h], kv_recv.at[p, i], sp, tp
+        )
+
+    @pl.loop(0, n_tp)
+    def _(i):
+        rows = pl.ds(pl.multiple_of(i * size, size), size)
+        pltpu.make_async_copy(tokens.at[rows], xbuf.at[t, rows], own_sem.at[i]).wait()
+        token_copy(0, i).wait_recv()
+        token_copy(2, i).start()
+        token_copy(1, i).wait_recv()
+        token_copy(2, i).wait_recv()
+
+        @pl.loop(0, size // step)
+        def _(k):
+            place = pl.ds(pl.multiple_of(i * size + k * step, step), step)
+            total = jnp.zeros((step, 1), jnp.float32)
+            for part in range(n_tp):
+                x = xbuf[part, place, :].astype(jnp.float32)
+                total = total + jnp.sum(x * x, axis=1, keepdims=True)
+                columns = slice(part * shard, (part + 1) * shard)
+                scaled[place, columns] = (x * gain[:, columns]).astype(jnp.bfloat16)
+            inverse[place, :] = lax.rsqrt(total * (1.0 / model) + epsilon)
+
+        x = scaled[rows, :]
+        inv = inverse[rows, :]
+
+        def project(index):
+            y_ = jnp.dot(x, weights[index], preferred_element_type=jnp.float32)
+            return (y_ * inv).astype(jnp.bfloat16)
+
+        k_rows = jnp.dot(order, project(0), preferred_element_type=jnp.float32)
+        q_rows = jnp.dot(order, project(1), preferred_element_type=jnp.float32) * (HEAD_DIM**-0.5)
+        v_cols = jnp.dot(order, project(2), preferred_element_type=jnp.float32).T
+        bias_rows = jnp.dot(bias[:, rows], back, preferred_element_type=jnp.float32)
+        pair_width = 2 * HEAD_DIM
+        for h in range(heads):
+            pair = slice((h // 2) * pair_width, (h // 2 + 1) * pair_width)
+            kp, qp = k_rows[:, pair], q_rows[:, pair]
+            if h % 2 == 0:
+                kq = jnp.where(lane < HEAD_DIM, kp, pltpu.roll(qp, HEAD_DIM, 1))
+            else:
+                kq = jnp.where(lane < HEAD_DIM, pltpu.roll(kp, HEAD_DIM, 1), qp)
+            kq = kq.astype(jnp.bfloat16)
+            vb = v_cols[h * HEAD_DIM : (h + 1) * HEAD_DIM, :].astype(jnp.bfloat16)
+            row = lax.broadcasted_iota(jnp.int32, (16, 128), 0)
+            tail = jnp.where(row == 0, bias_rows[h : h + 1, :128], 0.0)
+            tail = jnp.where(row == 1, bias_rows[h : h + 1, 128:], tail).astype(jnp.bfloat16)
+
+            def put(ref):
+                ref[0:size, :] = kq
+                ref[size : size + HEAD_DIM, :] = vb[:, :128]
+                ref[size + HEAD_DIM : size + 2 * HEAD_DIM, :] = vb[:, 128:]
+                ref[size + 2 * HEAD_DIM :, :] = tail
+
+            put(outgoing.at[i, h])
+
+            @pl.when(c * heads + h == p)
+            def _():
+                put(gathered.at[p, i])
+
+            kv_copy(i, h).start()
+
+    for load in loads[3:6]:
+        load.wait()
+
+    def gate(u):
+        rows = pl.ds(u * size, size)
+        x = scaled[rows, :]
+        inv = inverse[rows, :]
+        outs = []
+        for index in range(3, 6):
+            y_ = jnp.dot(x, weights[index], preferred_element_type=jnp.float32)
+            outs.append((y_ * inv).astype(jnp.bfloat16))
+        product[pl.ds(8 + u * size, size), :] = outs[1].astype(jnp.float32) * outs[0].astype(jnp.float32)
+        ready[rows, :] = outs[2]
+
+    gate(n_tp - 1)
+    rim_out[...] = product[pl.ds(tok_dev, 8), :]
+    rim_copy = remote(rim_out, rim, rim_sem.at[0], rim_sem.at[1], (p + 1) % n_sp, t)
+    rim_copy.start()
+    for u in range(n_tp - 1):
+        gate(u)
+    rim_copy.wait()
+    product[0:8, :] = jnp.where(p > 0, rim[...], 0.0)
+    tap_values = taps[...].astype(jnp.float32)
+
+    def filt_copy(u):
+        return remote(ready.at[pl.ds(u * size, size)], filt.at[t], filt_send.at[u], filt_recv.at[t], p, u)
+
+    for u in range(n_tp):
+        running = jnp.zeros((size, width), jnp.float32)
+        for w in range(CONV_W):
+            start = 8 - (CONV_W - 1) + w + u * size
+            running = running + tap_values[w : w + 1, :] * product[pl.ds(start, size), :]
+        rows = pl.ds(u * size, size)
+        done = (ready[rows, :].astype(jnp.float32) * running).astype(jnp.bfloat16)
+        ready[rows, :] = done
+
+        @pl.when(t == u)
+        def _():
+            filt[u] = done
+
+        @pl.when(t != u)
+        def _():
+            filt_copy(u).start()
+
+    row16 = lax.broadcasted_iota(jnp.int32, (16, 128), 0)
+    lane16 = lax.broadcasted_iota(jnp.int32, (16, 128), 1)
+    units = [
+        jnp.where((row16 == k) & (lane16 == HEAD_DIM), 1.0, 0.0).astype(jnp.bfloat16) for k in range(2)
+    ]
+    constant = jnp.where(lane == HEAD_DIM, 1.0, 0.0)
+
+    def arrival(b, i):
+        return remote(outgoing.at[i, 0], gathered.at[b, i], fwd_send.at[b, i], kv_recv.at[b, i], p, mate)
+
+    def forward(b, i):
+        return remote(gathered.at[b, i], gathered.at[b, i], fwd_send.at[b, i], kv_recv.at[b, i], p, mate)
+
+    def take(base):
+        @pl.loop(0, n_tp)
+        def _(i):
+            @pl.loop(0, half_sp)
+            def _(k):
+                b = base + k
+
+                @pl.when(jnp.logical_not(primary & (b == p)))
+                def _():
+                    arrival(b, i).wait_recv()
+
+                @pl.when(primary & (b != p))
+                def _():
+                    forward(b, i).start()
+
+                kq = gathered[b, i, 0:size, :].astype(jnp.float32)
+                tail = gathered[b, i, size + 2 * HEAD_DIM :, :]
+                column = jnp.concatenate(
+                    [
+                        lax.dot_general(
+                            tail, unit, (((0,), (0,)), ((), ())), preferred_element_type=jnp.float32
+                        )
+                        for unit in units
+                    ],
+                    axis=0,
+                )
+                keys[b, i] = jnp.where(lane < HEAD_DIM, kq, column).astype(jnp.bfloat16)
+
+                @pl.when(tile_core(i) == c)
+                def _():
+                    index = b * (n_tp // 2) + i // 2
+                    rolled = pltpu.roll(kq, HEAD_DIM, 1)
+                    quer[index] = jnp.where(lane < HEAD_DIM, rolled, constant).astype(jnp.bfloat16)
+
+    col = lax.broadcasted_iota(jnp.int32, (8, size), 1)
+    place8 = (col % 8) * groups + (groups - 1) - col // 8
+    relative = place8 - lax.broadcasted_iota(jnp.int32, (8, size), 0) * groups
+    wb, rb = (w0, w1), (r0, r1)
+
+    def early(slot, index, b, masked):
+        q = quer[index]
+        tile = tile_at(index, c)
+        for s in range(n_tp):
+            scores = lax.dot_general(
+                keys[b, s], q, (((1,), (1,)), ((), ())), preferred_element_type=jnp.float32
+            )
+            shift = (tile % n_tp - s) * size
+            run = None
+            for j in range(groups):
+                e = jnp.exp(jnp.minimum(scores[8 * j : 8 * j + 8, :], score_cap_fast))
+                if masked:
+                    e = jnp.where(relative + shift > groups - 1 - j, e, 0.0)
+                r = 1.0 / (1.0 + e)
+                run = r if run is None else run * r
+                w = e * run
+                if j % 2:
+                    pair = jnp.concatenate([before, w], axis=0).astype(jnp.bfloat16)
+                    wb[slot][s, 8 * (j - 1) : 8 * (j + 1), :] = pair
+                before = w
+            rb[slot][s] = run
+
+    def late(slot, index, b):
+        first = b == tile_at(index, c) // n_tp
+        running = jnp.where(first, 1.0, carry[index])
+        total = jnp.where(first, 0.0, acc[index])
+        for s in range(n_tp - 1, -1, -1):
+            run = rb[slot][s]
+            factor = later_product(run) * running
+            running = jnp.broadcast_to((factor * run)[:1], run.shape)
+            twice = jnp.concatenate([factor, factor], axis=0).astype(jnp.bfloat16)
+            pieces = [wb[slot][s, 16 * j : 16 * j + 16, :] * twice for j in range(groups // 2)]
+            values = jnp.concatenate(
+                [
+                    gathered[b, s, size : size + HEAD_DIM, :],
+                    gathered[b, s, size + HEAD_DIM : size + 2 * HEAD_DIM, :],
+                ],
+                axis=1,
+            )
+            total = total + jnp.dot(
+                values, jnp.concatenate(pieces, axis=0), preferred_element_type=jnp.float32
+            )
+        acc[index] = total
+        carry[index] = running
+
+    def tile_copy(index):
+        tile = tile_at(index, c)
+        b, u = tile // n_tp, tile % n_tp
+        return remote(tiles.at[index], arrived.at[head], a_send.at[index], a_recv.at[head], b, u)
+
+    def mark_copy(index):
+        tile = tile_at(index, c)
+        b, u = tile // n_tp, tile % n_tp
+        slot = p % heads * n_tp + u
+        return remote(mass.at[index], marks.at[slot], m_send.at[index], m_recv.at[slot], b, owner)
+
+    def ownership(index):
+        tile = tile_at(index, c)
+        b, u = tile // n_tp, tile % n_tp
+        return u, (b == p) & (u == t), (b == p) & (owner == t)
+
+    def hand_over(index):
+        u, own_tile, own_mark = ownership(index)
+        value = acc[index].astype(jnp.bfloat16)
+        mark = jnp.log(jnp.maximum(1.0 - carry[index], mass_floor))
+        tiles[index] = value
+        mass[index] = mark
+
+        @pl.when(own_tile)
+        def _():
+            arrived[head] = value
+
+        @pl.when(jnp.logical_not(own_tile))
+        def _():
+            tile_copy(index).start()
+
+        @pl.when(own_mark)
+        def _():
+            marks[p % heads * n_tp + u] = mark
+
+        @pl.when(jnp.logical_not(own_mark))
+        def _():
+            mark_copy(index).start()
+
+    half_tiles = n_tiles // 2
+    per_block = n_tp // 2
+
+    def block_of(index):
+        return tile_at(index, c) // n_tp
+
+    def sweep(base, from_diagonal, low, items, sends):
+        steps = items + 1
+        skip = steps % 2
+        spare = jnp.int32(n_tiles)
+
+        def start_of(index):
+            return jnp.where(from_diagonal, block_of(index), half_sp - 1)
+
+        def half(z, m, state):
+            i1, b1, i2, b2 = state
+
+            def go(masked):
+                late(z, i2, b2)
+                early(1 - z, i1, b1, masked)
+
+            lax.cond(b1 == block_of(i1), lambda: go(True), lambda: go(False))
+
+            @pl.when(sends & (b2 == 0) & (m >= 1))
+            def _():
+                hand_over(i2)
+
+            last = b1 == low
+            after = jnp.minimum(i1 + 1, base + half_tiles - 1)
+            ni = jnp.where(last, after, i1)
+            nb = jnp.where(last, start_of(after), b1 - 1)
+            advance = m >= 0
+            return (
+                jnp.where(advance, ni, i1),
+                jnp.where(advance, nb, b1),
+                jnp.where(advance, i1, spare),
+                b1,
+            )
+
+        def body(k, state):
+            for z in range(2):
+                state = half(z, 2 * k + z - skip, state)
+            return state
+
+        first = start_of(base)
+        rounds = jnp.where(items > 0, (steps + skip) // 2, 0)
+        lax.fori_loop(0, rounds, body, (base, first, spare, first))
+
+    triangle = per_block * (half_sp * (half_sp + 1) // 2)
+    square = per_block * half_sp * half_sp
+    is_upper = upper == 1
+
+    @pl.loop(0, 3)
+    def _(phase):
+        near = phase == 0
+
+        @pl.when(near)
+        def _():
+            take(upper * half_sp)
+
+        @pl.when(phase == 1)
+        def _():
+            loads[6].wait()
+            for k in range(1, n_tp):
+                u = (t + k) % n_tp
+                remote(ready.at[pl.ds(0, size)], filt.at[u], filt_send.at[u], filt_recv.at[u], p, u).wait()
+
+            @pl.loop(0, model // 256)
+            def _(k):
+                at = pl.ds(pl.multiple_of(k * 256, 256), 256)
+                total = jnp.zeros((size, 256), jnp.float32)
+                for part in range(n_tp):
+                    total = total + jnp.dot(
+                        filt[part],
+                        wf[part * width : (part + 1) * width, at],
+                        preferred_element_type=jnp.float32,
+                    )
+                partial[:, at] = total
+
+            take((1 - upper) * half_sp)
+
+        first_items = jnp.where(is_upper, square, triangle + square)
+        last_items = jnp.where(is_upper, triangle, 0)
+        sweep(
+            jnp.where(near, upper * half_tiles, jnp.where(phase == 1, half_tiles, 0)),
+            jnp.logical_not(is_upper & (phase == 1)),
+            jnp.where(near, upper * half_sp, 0),
+            jnp.where(near, triangle, jnp.where(phase == 1, first_items, last_items)),
+            jnp.logical_not(near & is_upper),
+        )
+
+    loads[7].wait()
+    mine = tile_core(t) == c
+
+    @pl.loop(0, total_heads)
+    def _(k):
+        @pl.when(jnp.logical_not((k == head) & mine))
+        def _():
+            remote(tiles.at[0], arrived.at[k], a_send.at[0], a_recv.at[k], p, t).wait_recv()
+
+    for part in range(n_tp):
+        stack = jnp.concatenate([arrived[part * heads + h] for h in range(heads)], axis=0)
+        rows = lax.dot_general(back, stack, (((1,), (1,)), ((), ())), preferred_element_type=jnp.float32)
+        attended[:, part * width : (part + 1) * width] = rows.astype(jnp.bfloat16)
+
+    @pl.loop(0, model // 256)
+    def _(k):
+        at = pl.ds(pl.multiple_of(k * 256, 256), 256)
+        total = partial[:, at] + jnp.dot(attended[...], wa[:, at], preferred_element_type=jnp.float32)
+        mixed[:, at] = total.astype(jnp.bfloat16)
+
+    @pl.loop(0, heads)
+    def _(h):
+        for u in range(n_tp):
+            own_mark = (p == c * heads + h) & (tile_core(u) == c)
+
+            @pl.when(jnp.logical_not(own_mark))
+            def _():
+                slot = h * n_tp + u
+                remote(mass.at[0], marks.at[slot], m_send.at[0], m_recv.at[slot], p, t).wait_recv()
+
+    for u in range(n_tp):
+        row = lax.broadcasted_iota(jnp.int32, (8, size), 0)
+        value = jnp.zeros((8, size), jnp.float32)
+        for h in range(heads):
+            value = jnp.where(row == h, marks[h * n_tp + u], value)
+        total = jnp.zeros((8, size), jnp.float32)
+        for _ in range(3):
+            high = value.astype(jnp.bfloat16)
+            value = value - high.astype(jnp.float32)
+            total = total + jnp.dot(high, order, preferred_element_type=jnp.float32)
+        logs[:, u * size : (u + 1) * size] = total[:heads]
+
+    @pl.loop(0, n_tiles)
+    def _(index):
+        u, own_tile, own_mark = ownership(index)
+
+        @pl.when(jnp.logical_not(own_tile))
+        def _():
+            tile_copy(index).wait_send()
+
+        @pl.when(jnp.logical_not(own_mark))
+        def _():
+            mark_copy(index).wait_send()
+
+    @pl.when(primary)
+    def _():
+        @pl.loop(0, n_tp)
+        def _(i):
+            @pl.loop(1, n_sp)
+            def _(k):
+                forward((p + k) % n_sp, i).wait_send()
+
+    for i in range(n_tp):
+        for kind in range(3):
+            token_copy(kind, i).wait_send()
+        for h in range(heads):
+            kv_copy(i, h).wait_send()
+
+
+def per_device_fast(
+    tokens,
+    norm_gain,
+    signal_proj,
+    postgate_proj,
+    pregate_proj,
+    query_proj,
+    key_proj,
+    value_proj,
+    filter_taps,
+    break_bias,
+    filter_readout,
+    attention_readout,
+):
+    n_sp, n_tp = lax.axis_size("sp"), lax.axis_size("tp")
+    tok_dev, shard = tokens.shape
+    heads = break_bias.shape[1]
+    width = key_proj.shape[1]
+    model = n_tp * shard
+    size = tok_dev // n_tp
+    block = size + 2 * HEAD_DIM + 16
+    n_tiles = n_sp * n_tp // 2
+    vmem = pl.BlockSpec(memory_space=pltpu.VMEM)
+    anywhere = pl.BlockSpec(memory_space=pl.ANY)
+    dma = pltpu.SemaphoreType.DMA
+    bf16, f32 = jnp.bfloat16, jnp.float32
+    return pl.pallas_call(
+        functools.partial(layer_kernel, n_sp, heads),
+        out_shape=[
+            jax.ShapeDtypeStruct((size, model), bf16),
+            jax.ShapeDtypeStruct((heads, tok_dev), f32),
+        ],
+        in_specs=[anywhere, vmem] + [anywhere] * 6 + [vmem, vmem, anywhere, anywhere],
+        out_specs=[vmem, vmem],
+        scratch_shapes=[
+            pltpu.VMEM((n_tp, tok_dev, shard), bf16),
+            pltpu.VMEM((tok_dev, model), bf16),
+            pltpu.VMEM((tok_dev, 1), f32),
+            pltpu.VMEM((6, model, width), bf16),
+            pltpu.VMEM((n_tp, heads, block, 128), bf16),
+            pltpu.VMEM((n_sp, n_tp, block, 128), bf16),
+            pltpu.VMEM((tok_dev + 8, width), f32),
+            pltpu.VMEM((8, width), f32),
+            pltpu.VMEM((8, width), f32),
+            pltpu.VMEM((tok_dev, width), bf16),
+            pltpu.VMEM((n_tp, size, width), bf16),
+            pltpu.VMEM((n_sp, n_tp, size, 128), bf16),
+            pltpu.VMEM((n_tiles, size, 128), bf16),
+            pltpu.VMEM((n_tiles + 1, HEAD_DIM, size), f32),
+            pltpu.VMEM((n_tiles + 1, 8, size), f32),
+            pltpu.VMEM((n_tp, size, size), bf16),
+            pltpu.VMEM((n_tp, size, size), bf16),
+            pltpu.VMEM((n_tp, 8, size), f32),
+            pltpu.VMEM((n_tp, 8, size), f32),
+            pltpu.VMEM((n_tiles, HEAD_DIM, size), bf16),
+            pltpu.VMEM((n_tiles, 8, size), f32),
+            pltpu.VMEM((heads * n_tp, HEAD_DIM, size), bf16),
+            pltpu.VMEM((heads * n_tp, 8, size), f32),
+            pltpu.VMEM(filter_readout.shape, bf16),
+            pltpu.VMEM(attention_readout.shape, bf16),
+            pltpu.VMEM((size, model), f32),
+            pltpu.VMEM((size, n_tp * width), bf16),
+            dma((8,)),
+            dma((n_tp,)),
+            dma((3, n_tp)),
+            dma((3, n_tp)),
+            dma((n_tp, heads)),
+            dma((n_sp, n_tp)),
+            dma((n_sp, n_tp)),
+            dma((2,)),
+            dma((n_tp,)),
+            dma((n_tp,)),
+            dma((n_tiles,)),
+            dma((heads * n_tp,)),
+            dma((n_tiles,)),
+            dma((heads * n_tp,)),
+        ],
+        compiler_params=pltpu.CompilerParams(
+            collective_id=0, has_side_effects=True, vmem_limit_bytes=60 * 1024 * 1024
+        ),
+        name="layer",
+    )(
+        tokens,
+        norm_gain.reshape(1, model),
+        signal_proj,
+        postgate_proj,
+        pregate_proj,
+        query_proj,
+        key_proj,
+        value_proj,
+        filter_taps,
+        break_bias.T,
+        filter_readout,
+        attention_readout,
+    )
+
+
+def per_device_any(*operands):
+    tok_dev = operands[0].shape[0]
+    heads_dev = operands[9].shape[1]
+    n_sp, n_tp = lax.axis_size("sp"), lax.axis_size("tp")
+    fast = n_tp == 4 and n_sp == 2 * heads_dev and tok_dev == n_tp * 256 and operands[6].shape[1] == 256
+    return (per_device_fast if fast else per_device)(*operands)
+
+
 def solution(mesh):
     placed = (
         P("sp", "tp"),
@@ -225,7 +910,7 @@
         P(),
     )
     return jax.shard_map(
-        per_device,
+        per_device_any,
         mesh=mesh,
         in_specs=placed,
         out_specs=(P(("sp", "tp"), None), P("tp", "sp")),

time: 342 us -> 123 us (0.36); the launches traced: 336 us -> 122 us
  waiting for transfers between devices: 120 us -> 0 us
  matrix products: 29.5 us -> 0 us
  starting transfers between devices: 24.4 us -> 0 us
  blocking collectives: 22.2 us -> 0 us
  between operations: 14.3 us -> 0.64 us
  Pallas kernels: 107 us -> 118 us
  other arithmetic: 8.11 us -> 0 us
  local copies, waits for them, and re-layouts: 10.6 us -> 3.63 us
    ppermute x2 -> x0, waiting for transfers between devices: 55.9 us -> none  [passed_along(): return lax.ppermute(block, axis, route)]
    all_gather x1 -> x0, waiting for transfers between devices: 39.4 us -> none  [per_device(): whole_rows = lax.all_gather(tokens, 'tp', axis=1, tiled=True)]
    dot_general x7 -> x0, matrix products: 29.5 us -> none  [the longest x5 19.6 us: project(): product = jnp.dot(scaled, weight, preferred_element_type=jnp.float32)]
    all_to_all x4 -> x0, waiting for transfers between devices: 24.4 us -> none  [the longest x1 18.4 us: per_device(): lax.all_to_all(computed, 'sp', split_axis=0, concat_axis=0, tiled=True)]
    all_gather x1 -> x0, blocking collectives: 22.2 us -> none  [per_device(): all_bias = lax.all_gather(break_bias.T, 'sp', axis=1, tiled=True)]
    all_to_all x4 -> x0, starting transfers between devices: 18.2 us -> none  [the longest x1 5.61 us: per_device(): lax.all_to_all(outgoing, 'sp', split_axis=0, concat_axis=0, tiled=True)]
    pallas_call x1, Pallas kernels: 107 us -> 118 us  [per_device_fast(): pl.pallas_call(functools.partial(layer_kernel, n_sp, heads), out_shape=[j...]
    ppermute x2 -> x0, starting transfers between devices: 6.17 us -> none  [passed_along(): return lax.ppermute(block, axis, route)]
  transfers between devices with their start and end apart: 7 -> 0, of which waited for: 4 -> 0; matrix products, arithmetic and copies ran while one was open for 7% -> 0% of each run, Pallas kernels for 32% -> 0%
where the time goes in v2:
time: 123 us; the launch traced here: 122 us
  Pallas kernels  118 us (96%)
  local copies, waits for them, and re-layouts  3.63 us (3%)
    pallas_call x1, Pallas kernels, per_device_fast(): pl.pallas_call(functools.partial(layer_kernel, n_sp, heads), out_shape=[j...  118 us
    unnamed x2, local copies, waits for them, and re-layouts  3.63 us

profile of v2, /device:TPU:15, one launch (start us, length us, event | category | flops | bytes accessed | tf_op | source)
XLA Modules:
  0.0 122.4 jit_solution(13678494122307880866)
XLA Ops:
  0.6 118.2 %layer.1 = (bf16[256,2048]{1,0:T(8,128)(2,1)}, f32[4,1024]{1,0:T(4,128)}) custom-call(bf16[1024,512]{1,0:T(8,128)(2,1)} %tokens.1, f32[1,2048]{1,0:T(1,128)} %bitcast.2, bf16[2048,256]{1,0:T(8,128)(2,1)} %signal_w.1, bf16[2048,256]{1,0:T(8,128)(2,1)} %post_w.1, bf16[2048,256]{1,0:T(8,128)(2,1)} %pre_w.1, bf16[2048,256]{1,0:T(8,128)(2,1)} %query_w.1, ...), custom_call_target="tpu_custom_call" | custom-call | tf_op jit(solution)/shard_map/layer/pallas_call | solution.py:818
  118.8 2.3 %copy.16 = bf16[256,2048]{1,0:T(8,128)(2,1)} copy(bf16[256,2048]{1,0:T(8,128)(2,1)} %get-tuple-element.4) | data formatting | bytes 2097152
  121.1 1.3 %copy.17 = f32[4,1024]{1,0:T(4,128)} copy(f32[4,1024]{1,0:T(4,128)} %get-tuple-element.5) | data formatting | bytes 32768

commit v3 on v2

--- a/solution.py
+++ b/solution.py
@@ -277,7 +277,7 @@
     logs,
     xbuf,
     scaled,
-    inverse,
+    squares,
     weights,
     outgoing,
     gathered,
@@ -294,6 +294,8 @@
     w1,
     r0,
     r1,
+    s0,
+    s1,
     tiles,
     mass,
     arrived,
@@ -374,7 +376,7 @@
         copy.start()
     for load in loads[3:]:
         load.start()
-    for load in loads[:3]:
+    for load in loads[:6]:
         load.wait()
     order = scatter_matrix(False, size)
     back = scatter_matrix(True, size)
@@ -390,6 +392,82 @@
             outgoing.at[i, h], gathered.at[p, i], kv_send.at[i, h], kv_recv.at[p, i], sp, tp
         )
 
+    row16 = lax.broadcasted_iota(jnp.int32, (16, 128), 0)
+    lane16 = lax.broadcasted_iota(jnp.int32, (16, 128), 1)
+    units = [
+        jnp.where((row16 == k) & (lane16 == HEAD_DIM), 1.0, 0.0).astype(jnp.bfloat16) for k in range(2)
+    ]
+    constant = jnp.where(lane == HEAD_DIM, 1.0, 0.0)
+
+    def arrival(b, i):
+        return remote(outgoing.at[i, 0], gathered.at[b, i], fwd_send.at[b, i], kv_recv.at[b, i], p, mate)
+
+    def forward(b, i):
+        return remote(gathered.at[b, i], gathered.at[b, i], fwd_send.at[b, i], kv_recv.at[b, i], p, mate)
+
+    def accept(base, i):
+        @pl.loop(0, half_sp)
+        def _(k):
+            b = base + k
+
+            @pl.when(jnp.logical_not(primary & (b == p)))
+            def _():
+                arrival(b, i).wait_recv()
+
+            @pl.when(primary & (b != p))
+            def _():
+                forward(b, i).start()
+
+        for k in range(half_sp):
+            b = base + k
+            kq = gathered[b, i, 0:size, :].astype(jnp.float32)
+            tail = gathered[b, i, size + 2 * HEAD_DIM :, :]
+            column = jnp.concatenate(
+                [
+                    lax.dot_general(tail, unit, (((0,), (0,)), ((), ())), preferred_element_type=jnp.float32)
+                    for unit in units
+                ],
+                axis=0,
+            )
+            keys[b, i] = jnp.where(lane < HEAD_DIM, kq, column).astype(jnp.bfloat16)
+
+        @pl.when(tile_core(i) == c)
+        def _():
+            for k in range(half_sp):
+                b = base + k
+                index = b * (n_tp // 2) + i // 2
+                rolled = pltpu.roll(gathered[b, i, 0:size, :].astype(jnp.float32), HEAD_DIM, 1)
+                quer[index] = jnp.where(lane < HEAD_DIM, rolled, constant).astype(jnp.bfloat16)
+
+    tap_values = taps[...].astype(jnp.float32)
+    rim_copy = remote(rim_out, rim, rim_sem.at[0], rim_sem.at[1], (p + 1) % n_sp, t)
+
+    def gate(i, x, inv):
+        outs = []
+        for index in range(3, 6):
+            y_ = jnp.dot(x, weights[index], preferred_element_type=jnp.float32)
+            outs.append((y_ * inv).astype(jnp.bfloat16))
+        at = pl.ds(pl.multiple_of(8 + i * size, 8), size)
+        product[at, :] = outs[1].astype(jnp.float32) * outs[0].astype(jnp.float32)
+        ready[pl.ds(pl.multiple_of(i * size, size), size), :] = outs[2]
+
+    def convolve(i):
+        around = product[pl.ds(pl.multiple_of(i * size, size), size + 8), :]
+        running = jnp.zeros((size, width), jnp.float32)
+        for w in range(CONV_W):
+            start = 8 - (CONV_W - 1) + w
+            running = running + tap_values[w : w + 1, :] * around[start : start + size, :]
+        rows = pl.ds(pl.multiple_of(i * size, size), size)
+        done = (ready[rows, :].astype(jnp.float32) * running).astype(jnp.bfloat16)
+        ready[rows, :] = done
+
+        @pl.when(t == i)
+        def _():
+            filt[i] = done
+
+    def filt_copy(u):
+        return remote(ready.at[pl.ds(u * size, size)], filt.at[t], filt_send.at[u], filt_recv.at[t], p, u)
+
     @pl.loop(0, n_tp)
     def _(i):
         rows = pl.ds(pl.multiple_of(i * size, size), size)
@@ -400,18 +478,21 @@
         token_copy(2, i).wait_recv()
 
         @pl.loop(0, size // step)
-        def _(k):
-            place = pl.ds(pl.multiple_of(i * size + k * step, step), step)
-            total = jnp.zeros((step, 1), jnp.float32)
+        def _(k0):
+            place = pl.ds(pl.multiple_of(i * size + k0 * step, step), step)
+            total = jnp.zeros((step, 128), jnp.float32)
             for part in range(n_tp):
                 x = xbuf[part, place, :].astype(jnp.float32)
-                total = total + jnp.sum(x * x, axis=1, keepdims=True)
+                square = x * x
+                for k in range(0, shard, 128):
+                    total = total + square[:, k : k + 128]
                 columns = slice(part * shard, (part + 1) * shard)
                 scaled[place, columns] = (x * gain[:, columns]).astype(jnp.bfloat16)
-            inverse[place, :] = lax.rsqrt(total * (1.0 / model) + epsilon)
+            squares[pl.ds(pl.multiple_of(k0 * step, step), step), :] = total
 
         x = scaled[rows, :]
-        inv = inverse[rows, :]
+        total = jnp.sum(squares[...], axis=1, keepdims=True)
+        inv = lax.rsqrt(total * (1.0 / model) + epsilon)
 
         def project(index):
             y_ = jnp.dot(x, weights[index], preferred_element_type=jnp.float32)
@@ -449,109 +530,53 @@
 
             kv_copy(i, h).start()
 
-    for load in loads[3:6]:
-        load.wait()
-
-    def gate(u):
-        rows = pl.ds(u * size, size)
-        x = scaled[rows, :]
-        inv = inverse[rows, :]
-        outs = []
-        for index in range(3, 6):
-            y_ = jnp.dot(x, weights[index], preferred_element_type=jnp.float32)
-            outs.append((y_ * inv).astype(jnp.bfloat16))
-        product[pl.ds(8 + u * size, size), :] = outs[1].astype(jnp.float32) * outs[0].astype(jnp.float32)
-        ready[rows, :] = outs[2]
-
-    gate(n_tp - 1)
-    rim_out[...] = product[pl.ds(tok_dev, 8), :]
-    rim_copy = remote(rim_out, rim, rim_sem.at[0], rim_sem.at[1], (p + 1) % n_sp, t)
-    rim_copy.start()
-    for u in range(n_tp - 1):
-        gate(u)
+        gate(i, x, inv)
+
+        @pl.when(i == n_tp - 1)
+        def _():
+            rim_out[...] = product[tok_dev : tok_dev + 8, :]
+            rim_copy.start()
+
+        @pl.when(i > 0)
+        def _():
+            convolve(i)
+
+        @pl.when(i >= 2)
+        def _():
+            accept(upper * half_sp, i - 2)
+
+    for u in range(1, n_tp):
+
+        @pl.when(t != u)
+        def _():
+            filt_copy(u).start()
+
+    @pl.loop(n_tp - 2, n_tp)
+    def _(i):
+        accept(upper * half_sp, i)
+
     rim_copy.wait()
     product[0:8, :] = jnp.where(p > 0, rim[...], 0.0)
-    tap_values = taps[...].astype(jnp.float32)
-
-    def filt_copy(u):
-        return remote(ready.at[pl.ds(u * size, size)], filt.at[t], filt_send.at[u], filt_recv.at[t], p, u)
-
-    for u in range(n_tp):
-        running = jnp.zeros((size, width), jnp.float32)
-        for w in range(CONV_W):
-            start = 8 - (CONV_W - 1) + w + u * size
-            running = running + tap_values[w : w + 1, :] * product[pl.ds(start, size), :]
-        rows = pl.ds(u * size, size)
-        done = (ready[rows, :].astype(jnp.float32) * running).astype(jnp.bfloat16)
-        ready[rows, :] = done
-
-        @pl.when(t == u)
-        def _():
-            filt[u] = done
-
-        @pl.when(t != u)
-        def _():
-            filt_copy(u).start()
-
-    row16 = lax.broadcasted_iota(jnp.int32, (16, 128), 0)
-    lane16 = lax.broadcasted_iota(jnp.int32, (16, 128), 1)
-    units = [
-        jnp.where((row16 == k) & (lane16 == HEAD_DIM), 1.0, 0.0).astype(jnp.bfloat16) for k in range(2)
-    ]
-    constant = jnp.where(lane == HEAD_DIM, 1.0, 0.0)
-
-    def arrival(b, i):
-        return remote(outgoing.at[i, 0], gathered.at[b, i], fwd_send.at[b, i], kv_recv.at[b, i], p, mate)
-
-    def forward(b, i):
-        return remote(gathered.at[b, i], gathered.at[b, i], fwd_send.at[b, i], kv_recv.at[b, i], p, mate)
-
-    def take(base):
-        @pl.loop(0, n_tp)
-        def _(i):
-            @pl.loop(0, half_sp)
-            def _(k):
-                b = base + k
-
-                @pl.when(jnp.logical_not(primary & (b == p)))
-                def _():
-                    arrival(b, i).wait_recv()
-
-                @pl.when(primary & (b != p))
-                def _():
-                    forward(b, i).start()
-
-                kq = gathered[b, i, 0:size, :].astype(jnp.float32)
-                tail = gathered[b, i, size + 2 * HEAD_DIM :, :]
-                column = jnp.concatenate(
-                    [
-                        lax.dot_general(
-                            tail, unit, (((0,), (0,)), ((), ())), preferred_element_type=jnp.float32
-                        )
-                        for unit in units
-                    ],
-                    axis=0,
-                )
-                keys[b, i] = jnp.where(lane < HEAD_DIM, kq, column).astype(jnp.bfloat16)
-
-                @pl.when(tile_core(i) == c)
-                def _():
-                    index = b * (n_tp // 2) + i // 2
-                    rolled = pltpu.roll(kq, HEAD_DIM, 1)
-                    quer[index] = jnp.where(lane < HEAD_DIM, rolled, constant).astype(jnp.bfloat16)
+    convolve(0)
+
+    @pl.when(t != 0)
+    def _():
+        filt_copy(0).start()
 
     col = lax.broadcasted_iota(jnp.int32, (8, size), 1)
     place8 = (col % 8) * groups + (groups - 1) - col // 8
     relative = place8 - lax.broadcasted_iota(jnp.int32, (8, size), 0) * groups
-    wb, rb = (w0, w1), (r0, r1)
+    wb, rb, sb = (w0, w1), (r0, r1), (s0, s1)
+
+    def score(index, b, s):
+        return lax.dot_general(
+            keys[b, s], quer[index], (((1,), (1,)), ((), ())), preferred_element_type=jnp.float32
+        )
 
     def early(slot, index, b, masked):
-        q = quer[index]
         tile = tile_at(index, c)
         for s in range(n_tp):
-            scores = lax.dot_general(
-                keys[b, s], q, (((1,), (1,)), ((), ())), preferred_element_type=jnp.float32
-            )
+            scores = score(index, b, s) if s else sb[1 - slot]
             shift = (tile % n_tp - s) * size
             run = None
             for j in range(groups):
@@ -645,10 +670,16 @@
 
         def half(z, m, state):
             i1, b1, i2, b2 = state
+            last = b1 == low
+            after = jnp.minimum(i1 + 1, base + half_tiles - 1)
+            advance = m >= 0
+            ni = jnp.where(advance & last, after, i1)
+            nb = jnp.where(advance, jnp.where(last, start_of(after), b1 - 1), b1)
 
             def go(masked):
                 late(z, i2, b2)
                 early(1 - z, i1, b1, masked)
+                sb[1 - z][...] = score(ni, nb, 0)
 
             lax.cond(b1 == block_of(i1), lambda: go(True), lambda: go(False))
 
@@ -656,17 +687,7 @@
             def _():
                 hand_over(i2)
 
-            last = b1 == low
-            after = jnp.minimum(i1 + 1, base + half_tiles - 1)
-            ni = jnp.where(last, after, i1)
-            nb = jnp.where(last, start_of(after), b1 - 1)
-            advance = m >= 0
-            return (
-                jnp.where(advance, ni, i1),
-                jnp.where(advance, nb, b1),
-                jnp.where(advance, i1, spare),
-                b1,
-            )
+            return ni, nb, jnp.where(advance, i1, spare), b1
 
         def body(k, state):
             for z in range(2):
@@ -675,6 +696,7 @@
 
         first = start_of(base)
         rounds = jnp.where(items > 0, (steps + skip) // 2, 0)
+        sb[0][...] = score(base, first, 0)
         lax.fori_loop(0, rounds, body, (base, first, spare, first))
 
     triangle = per_block * (half_sp * (half_sp + 1) // 2)
@@ -684,10 +706,6 @@
     @pl.loop(0, 3)
     def _(phase):
         near = phase == 0
-
-        @pl.when(near)
-        def _():
-            take(upper * half_sp)
 
         @pl.when(phase == 1)
         def _():
@@ -708,7 +726,10 @@
                     )
                 partial[:, at] = total
 
-            take((1 - upper) * half_sp)
+            @pl.loop(0, n_tp)
+            def _(i):
+                accept((1 - upper) * half_sp, i)
+
 
         first_items = jnp.where(is_upper, square, triangle + square)
         last_items = jnp.where(is_upper, triangle, 0)
@@ -826,7 +847,7 @@
         scratch_shapes=[
             pltpu.VMEM((n_tp, tok_dev, shard), bf16),
             pltpu.VMEM((tok_dev, model), bf16),
-            pltpu.VMEM((tok_dev, 1), f32),
+            pltpu.VMEM((size, 128), f32),
             pltpu.VMEM((6, model, width), bf16),
             pltpu.VMEM((n_tp, heads, block, 128), bf16),
             pltpu.VMEM((n_sp, n_tp, block, 128), bf16),
@@ -843,6 +864,8 @@
             pltpu.VMEM((n_tp, size, size), bf16),
             pltpu.VMEM((n_tp, 8, size), f32),
             pltpu.VMEM((n_tp, 8, size), f32),
+            pltpu.VMEM((size, size), f32),
+            pltpu.VMEM((size, size), f32),
             pltpu.VMEM((n_tiles, HEAD_DIM, size), bf16),
             pltpu.VMEM((n_tiles, 8, size), f32),
             pltpu.VMEM((heads * n_tp, HEAD_DIM, size), bf16),

time: 123 us -> 116 us (0.943)
  Pallas kernels: 118 us -> 111 us
    pallas_call x1, Pallas kernels: 118 us -> 111 us  [per_device_fast(): pl.pallas_call(functools.partial(layer_kernel, n_sp, heads), out_shape=[j...]
where the time goes in v3:
time: 116 us
  Pallas kernels  111 us (96%)
  local copies, waits for them, and re-layouts  3.63 us (3%)
    pallas_call x1, Pallas kernels, per_device_fast(): pl.pallas_call(functools.partial(layer_kernel, n_sp, heads), out_shape=[j...  111 us
    unnamed x2, local copies, waits for them, and re-layouts  3.63 us

profile of v3, /device:TPU:15, one launch (start us, length us, event | category | flops | bytes accessed | tf_op | source)
XLA Modules:
  0.0 115.7 jit_solution(14747104461275047271)
XLA Ops:
  0.6 111.4 %layer.1 = (bf16[256,2048]{1,0:T(8,128)(2,1)}, f32[4,1024]{1,0:T(4,128)}) custom-call(bf16[1024,512]{1,0:T(8,128)(2,1)} %tokens.1, f32[1,2048]{1,0:T(1,128)} %bitcast.2, bf16[2048,256]{1,0:T(8,128)(2,1)} %signal_w.1, bf16[2048,256]{1,0:T(8,128)(2,1)} %post_w.1, bf16[2048,256]{1,0:T(8,128)(2,1)} %pre_w.1, bf16[2048,256]{1,0:T(8,128)(2,1)} %query_w.1, ...), custom_call_target="tpu_custom_call" | custom-call | tf_op jit(solution)/shard_map/layer/pallas_call | solution.py:839
  112.1 2.3 %copy.16 = bf16[256,2048]{1,0:T(8,128)(2,1)} copy(bf16[256,2048]{1,0:T(8,128)(2,1)} %get-tuple-element.4) | data formatting | bytes 2097152
  114.4 1.3 %copy.17 = f32[4,1024]{1,0:T(4,128)} copy(f32[4,1024]{1,0:T(4,128)} %get-tuple-element.5) | data formatting | bytes 32768
